TPU v7x, 512 devices: a whole 4x4x16 slice. The times are simulated.
512 devices in a mesh: sp: 256 (over z, y, x), tp: 2 (over core).
Axes of the slice: x: 4, y: 4, z: 16, core: 2. Of those that a mesh axis runs over, the one named last changes fastest.
Arguments:
- stream: bfloat16 [1024, 131072], P('tp', 'sp'), may hold values from -6 to 6
- norm_gain: float32 [2, 1024], replicated, may hold values from 0.1 to 1.9
- w_value: bfloat16 [2, 512, 1024], P(None, 'tp'), may hold values from -0.1875 to 0.1875
- w_gate: bfloat16 [2, 512, 1024], P(None, 'tp'), may hold values from -0.1875 to 0.1875
- conv_taps: bfloat16 [2, 512, 255], P(None, 'tp'), may hold values from -0.375 to 0.375
- group_gain: float32 [2, 512], P(None, 'tp'), may hold values from 0.1 to 1.9
- group_shift: float32 [2, 512], P(None, 'tp'), may hold values from -3 to 3
- w_out: bfloat16 [2, 1024, 512], P(None, 'tp'), may hold values from -0.25 to 0.25
Outputs:
- result: bfloat16 [1024, 131072], P('tp', 'sp')
All inputs are finite; a program needn't handle non-finite values.
Results may differ from a plain program's by a relative error of at most 0.014.
Values may be sent and summed in bfloat16 or wider, within the bound.
A program may use at most 64 MiB of HBM per device.

v0:
```python
import jax
import jax.numpy as jnp
from jax import lax
from jax.sharding import PartitionSpec as P

GROUP_DIM = 128


RMS_EPS = 1e-06
LN_EPS = 1e-05


def in_order(parts, dim):
    parts = jnp.moveaxis(parts, 0, dim)
    shape = parts.shape
    return parts.reshape(*shape[:dim], shape[dim] * shape[dim + 1], *shape[dim + 2 :])


def sent_to_all(value, axis):
    count = lax.axis_size(axis)
    return lax.all_to_all(
        jnp.broadcast_to(value[None], (count, *value.shape)), axis, 0, 0, tiled=True
    )


def gathered_copies(value, axis, dim):
    return in_order(sent_to_all(value, axis), dim)


def with_halo(cells, sides, width):
    for axis, dim in sides:
        count = lax.axis_size(axis)
        ends = count - 1
        head = lax.slice_in_dim(cells, 0, width, axis=dim)
        tail = lax.slice_in_dim(cells, cells.shape[dim] - width, cells.shape[dim], axis=dim)
        cells = jnp.concatenate(
            [
                lax.ppermute(tail, axis, [(i, (i + 1) % count) for i in range(ends)]),
                cells,
                lax.ppermute(head, axis, [((i + 1) % count, i) for i in range(ends)]),
            ],
            axis=dim,
        )
    return cells


def make_gated(whole, gain, value_weight, gate_weight):
    widened = whole.astype(jnp.float32)
    inverse_rms = lax.rsqrt(jnp.mean(widened * widened, axis=0, keepdims=True) + RMS_EPS)
    normed = (widened * inverse_rms * gain[:, None]).astype(jnp.bfloat16)
    projected = jnp.dot(value_weight, normed, preferred_element_type=jnp.float32).astype(
        jnp.bfloat16
    )
    gate_proj = jnp.dot(gate_weight, normed, preferred_element_type=jnp.float32).astype(
        jnp.bfloat16
    )
    return (projected.astype(jnp.float32) * jax.nn.sigmoid(gate_proj.astype(jnp.float32))).astype(
        jnp.bfloat16
    )


def filter_norm(padded, taps, ggain, gshift):
    channels = taps.shape[0]
    filtered = lax.conv_general_dilated(
        padded[None],
        taps[:, None, :],
        (1,),
        [(0, 0)],
        dimension_numbers=("NCW", "OIW", "NCW"),
        feature_group_count=channels,
        preferred_element_type=jnp.float32,
    )[0]
    tokens_here = filtered.shape[1]
    grouped = filtered.reshape(channels // GROUP_DIM, GROUP_DIM, tokens_here)
    group_mean = jnp.mean(grouped, axis=1, keepdims=True)
    centred = grouped - group_mean
    scaled = centred * lax.rsqrt(jnp.mean(centred * centred, axis=1, keepdims=True) + LN_EPS)
    scaled = scaled.reshape(channels, tokens_here) * ggain[:, None] + gshift[:, None]
    return jax.nn.silu(scaled).astype(jnp.bfloat16)


def body(stream, norm_gain, w_value, w_gate, conv_taps, group_gain, group_shift, w_out):
    rim_width = (conv_taps.shape[2] - 1) // 2
    layers = w_value.shape[0]
    for layer_index in range(layers):
        whole = gathered_copies(stream, "tp", 0)
        gated = make_gated(whole, norm_gain[layer_index], w_value[layer_index], w_gate[layer_index])
        padded = with_halo(gated, (("sp", 1),), rim_width)
        activated = filter_norm(
            padded, conv_taps[layer_index], group_gain[layer_index], group_shift[layer_index]
        )
        out_weight = w_out[layer_index]
        initial = jnp.zeros((out_weight.shape[0], activated.shape[1]), jnp.float32)
        branch = initial + jnp.dot(
            out_weight, gathered_copies(activated, "tp", 0), preferred_element_type=jnp.float32
        )
        stream = (stream.astype(jnp.float32) + branch).astype(jnp.bfloat16)
    return stream


def solution(mesh):
    placed = (
        P("tp", "sp"),
        P(),
        P(None, "tp", None),
        P(None, "tp", None),
        P(None, "tp", None),
        P(None, "tp"),
        P(None, "tp"),
        P(None, "tp", None),
    )
    return jax.shard_map(body, mesh=mesh, in_specs=placed, out_specs=P("tp", "sp"), check_vma=False)
```

profile of v0, /device:TPU:385, one launch (start us, length us, event | category | flops | bytes accessed | tf_op | source)
XLA Modules:
  0.0 111.9 jit_solution(7844882692543539370)
XLA Ops:
  0.0 2.1 %broadcast_in_dim.16 = bf16[2,512,512]{2,1,0:T(8,128)(2,1)} broadcast(bf16[512,512]{1,0:T(8,128)(2,1)} %param.8), dimensions={1,2} | broadcast | bytes 1572864 | tf_op jit(solution)/shard_map/broadcast_in_dim | solution.py:22
  2.1 4.4 %all-to-all-start = ((bf16[2,512,512]{2,1,0:T(8,128)(2,1)}), bf16[2,512,512]{2,1,0:T(8,128)(2,1)S(1)}, u32[]{:S(2)}, u32[]{:S(2)}) async-start(bf16[2,512,512]{2,1,0:T(8,128)(2,1)} %broadcast_in_dim.16), calls=%async_computation | async-start | bytes 2097152 | tf_op jit(solution)/shard_map/all_to_all | solution.py:21
  6.5 1.7 %all-to-all-done = bf16[2,512,512]{2,1,0:T(8,128)(2,1)S(1)} async-done(((bf16[2,512,512]{2,1,0:T(8,128)(2,1)}), bf16[2,512,512]{2,1,0:T(8,128)(2,1)S(1)}, u32[]{:S(2)}, u32[]{:S(2)}) %all-to-all-start) | async-done | bytes 1048608 | tf_op jit(solution)/shard_map/all_to_all | solution.py:21
  8.8 0.9 copy-done.5
  10.2 0.7 copy-done.7
  11.5 8.6 %collective-permute-start.1 = (bf16[256,127]{0,1:T(8,128)(2,1)S(1)}, bf16[256,127]{0,1:T(8,128)(2,1)S(1)}, u32[]{:S(2)}, u32[]{:S(2)}) collective-permute-start(bf16[256,127]{0,1:T(8,128)(2,1)S(1)} %get-tuple-element.10), channel_id=1, source_target_pairs={{2,0},{4,2},{6,4},{8,6},{10,8},{12,10},{14,12},{16,14},{18,16},{20... | collective-permute-start | bytes 195080 | tf_op jit(solution)/shard_map/ppermute | solution.py:40
  20.2 1.9 %collective-permute-start = (bf16[256,127]{0,1:T(8,128)(2,1)S(1)}, bf16[256,127]{0,1:T(8,128)(2,1)S(1)}, u32[]{:S(2)}, u32[]{:S(2)}) collective-permute-start(bf16[256,127]{0,1:T(8,128)(2,1)S(1)} %get-tuple-element.9), channel_id=1, source_target_pairs={{0,2},{2,4},{4,6},{6,8},{8,10},{10,12},{12,14},{14,16},{16,18},{18... | collective-permute-start | bytes 195080 | tf_op jit(solution)/shard_map/ppermute | solution.py:38
  23.1 7.5 %collective-permute-done = bf16[256,127]{0,1:T(8,128)(2,1)S(1)} collective-permute-done((bf16[256,127]{0,1:T(8,128)(2,1)S(1)}, bf16[256,127]{0,1:T(8,128)(2,1)S(1)}, u32[]{:S(2)}, u32[]{:S(2)}) %collective-permute-start) | collective-permute-done | bytes 65056 | tf_op jit(solution)/shard_map/ppermute | solution.py:38
  30.7 20.1 %fusion.30 = f32[1,256,512]{1,0,2:T(1,128)S(1)} fusion(bf16[256,1,255]{0,1,2:T(2,128)(2,1)S(1)} %copy.56, bf16[1,256,766]{1,2,0:T(8,128)(2,1)S(1)} %maximum_bitcast_fusion), kind=kOutput, calls=%fused_computation.40 | convolution fusion | flops 66846720 | bytes 1047040 | tf_op jit(solution)/shard_map/conv_general_dilated | solution.py:64
  50.8 0.7 copy.58
  51.4 0.6 reduce_sum.55
  52.1 1.6 %multiply_reduce_fusion.1 = f32[2,512]{0,1:T(8,128)S(1)} fusion(f32[2,128,512]{1,0,2:T(2,128)S(1)} %bitcast.105, f32[2,512]{0,1:T(8,128)S(1)} %broadcast_multiply_fusion.1), kind=kLoop, calls=%fused_computation.63 | loop fusion | flops 392192 | bytes 532480 | tf_op jit(solution)/shard_map/reduce_sum | solution.py:77
  54.4 5.7 %all_to_all.20 = bf16[2,256,512]{2,1,0:T(8,128)(2,1)S(1)} all-to-all(bf16[2,256,512]{2,1,0:T(8,128)(2,1)S(1)} %broadcast_in_dim.19), channel_id=1, replica_groups=mesh['sp'=256,'tp'=2] {'tp'}, dimensions={0} | all-to-all | bytes 1048576 | tf_op jit(solution)/shard_map/all_to_all | solution.py:21
  60.9 4.6 %all_to_all.21 = bf16[2,512,512]{2,1,0:T(8,128)(2,1)S(1)} all-to-all(bf16[2,512,512]{2,1,0:T(8,128)(2,1)S(1)} %broadcast_in_dim.20), channel_id=1, replica_groups=mesh['sp'=256,'tp'=2] {'tp'}, dimensions={0} | all-to-all | bytes 2097152 | tf_op jit(solution)/shard_map/all_to_all | solution.py:21
  66.2 0.9 copy-done.6
  67.6 0.7 copy-done.8
  68.9 1.9 %collective-permute-start.3 = (bf16[256,127]{0,1:T(8,128)(2,1)S(1)}, bf16[256,127]{0,1:T(8,128)(2,1)S(1)}, u32[]{:S(2)}, u32[]{:S(2)}) collective-permute-start(bf16[256,127]{0,1:T(8,128)(2,1)S(1)} %get-tuple-element.8), channel_id=1, source_target_pairs={{2,0},{4,2},{6,4},{8,6},{10,8},{12,10},{14,12},{16,14},{18,16},{20... | collective-permute-start | bytes 195080 | tf_op jit(solution)/shard_map/ppermute | solution.py:40
  70.8 3.4 %collective-permute-start.2 = (bf16[256,127]{0,1:T(8,128)(2,1)S(1)}, bf16[256,127]{0,1:T(8,128)(2,1)S(1)}, u32[]{:S(2)}, u32[]{:S(2)}) collective-permute-start(bf16[256,127]{0,1:T(8,128)(2,1)S(1)} %get-tuple-element.7), channel_id=1, source_target_pairs={{0,2},{2,4},{4,6},{6,8},{8,10},{10,12},{12,14},{14,16},{16,18},{18... | collective-permute-start | bytes 195080 | tf_op jit(solution)/shard_map/ppermute | solution.py:38
  74.5 6.7 %collective-permute-done.2 = bf16[256,127]{0,1:T(8,128)(2,1)S(1)} collective-permute-done((bf16[256,127]{0,1:T(8,128)(2,1)S(1)}, bf16[256,127]{0,1:T(8,128)(2,1)S(1)}, u32[]{:S(2)}, u32[]{:S(2)}) %collective-permute-start.2) | collective-permute-done | bytes 65056 | tf_op jit(solution)/shard_map/ppermute | solution.py:38
  81.3 20.1 %fusion.28 = f32[1,256,512]{1,0,2:T(1,128)S(1)} fusion(bf16[256,1,255]{0,1,2:T(2,128)(2,1)S(1)} %copy.63, bf16[1,256,766]{1,2,0:T(8,128)(2,1)S(1)} %maximum_bitcast_fusion.1), kind=kOutput, calls=%fused_computation.38 | convolution fusion | flops 66846720 | bytes 1047040 | tf_op jit(solution)/shard_map/conv_general_dilated | solution.py:64
  101.4 0.7 copy.65
  102.7 1.6 %multiply_reduce_fusion = f32[2,512]{0,1:T(8,128)S(1)} fusion(f32[2,128,512]{1,0,2:T(2,128)S(1)} %bitcast.103, f32[2,512]{0,1:T(8,128)S(1)} %broadcast_multiply_fusion), kind=kLoop, calls=%fused_computation.58 | loop fusion | flops 392192 | bytes 532480 | tf_op jit(solution)/shard_map/reduce_sum | solution.py:77
  105.0 5.4 %all_to_all.22 = bf16[2,256,512]{2,1,0:T(8,128)(2,1)S(1)} all-to-all(bf16[2,256,512]{2,1,0:T(8,128)(2,1)S(1)} %broadcast_in_dim.23), channel_id=1, replica_groups=mesh['sp'=256,'tp'=2] {'tp'}, dimensions={0} | all-to-all | bytes 1048576 | tf_op jit(solution)/shard_map/all_to_all | solution.py:21
  110.9 1.0 copy.67
  (66 shorter events, 8.0 us)
Async XLA Ops:
  2.1 4.4 %copy-start.2 = (f32[2,1024]{1,0:T(2,128)S(1)}, f32[2,1024]{1,0:T(2,128)}, u32[]{:S(2)}) copy-start(f32[2,1024]{1,0:T(2,128)} %param.9) | copy-start | bytes 24580
  2.1 6.1 %all-to-all-start = ((bf16[2,512,512]{2,1,0:T(8,128)(2,1)}), bf16[2,512,512]{2,1,0:T(8,128)(2,1)S(1)}, u32[]{:S(2)}, u32[]{:S(2)}) async-start(bf16[2,512,512]{2,1,0:T(8,128)(2,1)} %broadcast_in_dim.16), calls=%async_computation | async-start | bytes 2097152 | tf_op jit(solution)/shard_map/all_to_all | solution.py:21
  8.5 1.2 %copy-start.5 = (bf16[2,256,1024]{2,1,0:T(8,128)(2,1)S(1)}, bf16[2,256,1024]{2,1,0:T(8,128)(2,1)}, u32[]{:S(2)}) copy-start(bf16[2,256,1024]{2,1,0:T(8,128)(2,1)} %param.10) | copy-start | bytes 3145732
  9.7 1.2 %copy-start.7 = (bf16[2,256,1024]{2,1,0:T(8,128)(2,1)S(1)}, bf16[2,256,1024]{2,1,0:T(8,128)(2,1)}, u32[]{:S(2)}) copy-start(bf16[2,256,1024]{2,1,0:T(8,128)(2,1)} %param.11) | copy-start | bytes 3145732
  11.0 11.1 %copy-start.3 = (f32[2,256]{1,0:T(2,128)S(1)}, f32[2,256]{1,0:T(2,128)}, u32[]{:S(2)}) copy-start(f32[2,256]{1,0:T(2,128)} %param.14) | copy-start | bytes 6148
  11.0 11.1 %copy-start.1 = (bf16[2,256,255]{1,0,2:T(2,128)(2,1)S(1)}, bf16[2,256,255]{1,0,2:T(2,128)(2,1)}, u32[]{:S(2)}) copy-start(bf16[2,256,255]{1,0,2:T(2,128)(2,1)} %param.12) | copy-start | bytes 783364
  11.5 11.0 %copy-start.4 = (f32[2,256]{1,0:T(2,128)S(1)}, f32[2,256]{1,0:T(2,128)}, u32[]{:S(2)}) copy-start(f32[2,256]{1,0:T(2,128)} %param.13) | copy-start | bytes 6148
  11.5 11.0 %copy-start = (bf16[512,512]{1,0:T(8,128)(2,1)S(1)}, bf16[512,512]{1,0:T(8,128)(2,1)}, u32[]{:S(2)}) copy-start(bf16[512,512]{1,0:T(8,128)(2,1)} %param.8) | copy-start | bytes 1572868
  11.5 11.6 %collective-permute-start.1 = (bf16[256,127]{0,1:T(8,128)(2,1)S(1)}, bf16[256,127]{0,1:T(8,128)(2,1)S(1)}, u32[]{:S(2)}, u32[]{:S(2)}) collective-permute-start(bf16[256,127]{0,1:T(8,128)(2,1)S(1)} %get-tuple-element.10), channel_id=1, source_target_pairs={{2,0},{4,2},{6,4},{8,6},{10,8},{12,10},{14,12},{16,14},{18,16},{20... | collective-permute-start | bytes 195080 | tf_op jit(solution)/shard_map/ppermute | solution.py:40
  20.2 10.4 %collective-permute-start = (bf16[256,127]{0,1:T(8,128)(2,1)S(1)}, bf16[256,127]{0,1:T(8,128)(2,1)S(1)}, u32[]{:S(2)}, u32[]{:S(2)}) collective-permute-start(bf16[256,127]{0,1:T(8,128)(2,1)S(1)} %get-tuple-element.9), channel_id=1, source_target_pairs={{0,2},{2,4},{4,6},{6,8},{8,10},{10,12},{12,14},{14,16},{16,18},{18... | collective-permute-start | bytes 195080 | tf_op jit(solution)/shard_map/ppermute | solution.py:38
  54.4 5.8 %copy-start.9 = (bf16[2,512,512]{2,1,0:T(8,128)(2,1)S(1)}, bf16[2,512,512]{2,1,0:T(8,128)(2,1)}, u32[]{:S(2)}) copy-start(bf16[2,512,512]{2,1,0:T(8,128)(2,1)} %param.15) | copy-start | bytes 3145732
  65.9 1.2 %copy-start.6 = (bf16[2,256,1024]{2,1,0:T(8,128)(2,1)S(1)}, bf16[2,256,1024]{2,1,0:T(8,128)(2,1)}, u32[]{:S(2)}) copy-start(bf16[2,256,1024]{2,1,0:T(8,128)(2,1)} %param.10) | copy-start | bytes 3145732
  67.1 1.2 %copy-start.8 = (bf16[2,256,1024]{2,1,0:T(8,128)(2,1)S(1)}, bf16[2,256,1024]{2,1,0:T(8,128)(2,1)}, u32[]{:S(2)}) copy-start(bf16[2,256,1024]{2,1,0:T(8,128)(2,1)} %param.11) | copy-start | bytes 3145732
  68.9 5.7 %collective-permute-start.3 = (bf16[256,127]{0,1:T(8,128)(2,1)S(1)}, bf16[256,127]{0,1:T(8,128)(2,1)S(1)}, u32[]{:S(2)}, u32[]{:S(2)}) collective-permute-start(bf16[256,127]{0,1:T(8,128)(2,1)S(1)} %get-tuple-element.8), channel_id=1, source_target_pairs={{2,0},{4,2},{6,4},{8,6},{10,8},{12,10},{14,12},{16,14},{18,16},{20... | collective-permute-start | bytes 195080 | tf_op jit(solution)/shard_map/ppermute | solution.py:40
  70.8 10.4 %collective-permute-start.2 = (bf16[256,127]{0,1:T(8,128)(2,1)S(1)}, bf16[256,127]{0,1:T(8,128)(2,1)S(1)}, u32[]{:S(2)}, u32[]{:S(2)}) collective-permute-start(bf16[256,127]{0,1:T(8,128)(2,1)S(1)} %get-tuple-element.7), channel_id=1, source_target_pairs={{0,2},{2,4},{4,6},{6,8},{8,10},{10,12},{12,14},{14,16},{16,18},{18... | collective-permute-start | bytes 195080 | tf_op jit(solution)/shard_map/ppermute | solution.py:38
  105.0 5.4 %copy-start.10 = (bf16[2,512,512]{2,1,0:T(8,128)(2,1)S(1)}, bf16[2,512,512]{2,1,0:T(8,128)(2,1)}, u32[]{:S(2)}) copy-start(bf16[2,512,512]{2,1,0:T(8,128)(2,1)} %param.15) | copy-start | bytes 3145732
where the time goes:
time: 113 us; the launch traced here: 112 us
  matrix products  43.1 us (38%)
  starting transfers between devices  20.2 us (18%)
  waiting for transfers between devices  15.9 us (14%)
  blocking collectives  15.7 us (14%)
  local copies, waits for them, and re-layouts  10.2 us (9%)
  other arithmetic  6.41 us (6%)
    conv_general_dilated x2, matrix products, filter_norm(): lax.conv_general_dilated(padded[None], taps[:, None, :], (1,), [(0, 0)],...  40.1 us
    all_to_all x3, blocking collectives, sent_to_all(): lax.all_to_all(jnp.broadcast_to(value[None], (count, *value.shape)), axis...  15.7 us
    ppermute x2, waiting for transfers between devices, with_halo(): lax.ppermute(tail, axis, [(i, (i + 1) % count) for i in range(ends)])  14.2 us
    ppermute x2, starting transfers between devices, with_halo(): lax.ppermute(head, axis, [((i + 1) % count, i) for i in range(ends)])  10.5 us
    ppermute x2, starting transfers between devices, with_halo(): lax.ppermute(tail, axis, [(i, (i + 1) % count) for i in range(ends)])  5.28 us
    all_to_all x1, starting transfers between devices, sent_to_all(): lax.all_to_all(jnp.broadcast_to(value[None], (count, *value.shape)), axis...  4.37 us
    unnamed x27, local copies, waits for them, and re-layouts  4.11 us
    reduce_sum x2, other arithmetic, filter_norm(): jnp.mean(centred * centred, axis=1, keepdims=True) + LN_EPS  3.18 us
  transfers between devices with their start and end apart: 5, of which 3 were waited for; matrix products, arithmetic and copies ran while one was open for 1% of the time, Pallas kernels for 0%

commit v1 on v0

--- a/solution.py
+++ b/solution.py
@@ -1,5 +1,6 @@
 import jax
 import jax.numpy as jnp
+import numpy as np
 from jax import lax
 from jax.sharding import PartitionSpec as P
 
@@ -59,17 +60,26 @@
     )
 
 
+def trig_tables(size, rows, outputs):
+    freqs = (np.arange(size // 2) + 0.5) * (2 * np.pi / size)
+    angle = np.arange(rows)[:, None] * freqs[None]
+    forward = np.concatenate([np.cos(angle), np.sin(angle)], axis=1)
+    back = forward[:outputs].T
+    return jnp.asarray(forward, jnp.bfloat16), jnp.asarray(back, jnp.bfloat16)
+
+
 def filter_norm(padded, taps, ggain, gshift):
     channels = taps.shape[0]
-    filtered = lax.conv_general_dilated(
-        padded[None],
-        taps[:, None, :],
-        (1,),
-        [(0, 0)],
-        dimension_numbers=("NCW", "OIW", "NCW"),
-        feature_group_count=channels,
-        preferred_element_type=jnp.float32,
-    )[0]
+    window = padded.shape[1]
+    size = -(-window // 256) * 256
+    forward, inverse = trig_tables(size, size, window - taps.shape[1] + 1)
+    half = size // 2
+    spectrum = jnp.dot(padded, forward[:window], preferred_element_type=jnp.float32)
+    response = jnp.dot(taps, forward[: taps.shape[1]], preferred_element_type=jnp.float32) * (2.0 / size)
+    gr, gs = spectrum[:, :half], spectrum[:, half:]
+    hr, hs = response[:, :half], response[:, half:]
+    product = jnp.concatenate([gr * hr + gs * hs, gs * hr - gr * hs], axis=1).astype(jnp.bfloat16)
+    filtered = jnp.dot(product, inverse, preferred_element_type=jnp.float32)
     tokens_here = filtered.shape[1]
     grouped = filtered.reshape(channels // GROUP_DIM, GROUP_DIM, tokens_here)
     group_mean = jnp.mean(grouped, axis=1, keepdims=True)

time: 113 us -> 74.2 us (0.66)
  matrix products: 43.1 us -> 8.36 us
  waiting for transfers between devices: 15.9 us -> 9.49 us
  blocking collectives: 15.7 us -> 20.9 us
  other arithmetic: 6.41 us -> 1.84 us
  local copies, waits for them, and re-layouts: 10.2 us -> 13.3 us
    conv_general_dilated x2 -> x0, matrix products: 40.1 us -> none  [filter_norm(): lax.conv_general_dilated(padded[None], taps[:, None, :], (1,), [(0, 0)],...]
    dot_general x0 -> x12, matrix products: none -> 5.41 us  [the longest x6 3.59 us: filter_norm(): jnp.dot(padded, forward[:window], preferred_element_type=jnp.float32)]
    all_to_all x3 -> x4, blocking collectives: 15.7 us -> 20.9 us  [sent_to_all(): lax.all_to_all(jnp.broadcast_to(value[None], (count, *value.shape)), axis...]
    ppermute x2, starting transfers between devices: 10.5 us -> 15.3 us  [with_halo(): lax.ppermute(head, axis, [((i + 1) % count, i) for i in range(ends)])]
    ppermute x2, waiting for transfers between devices: 14.2 us -> 9.48 us  [with_halo(): lax.ppermute(tail, axis, [(i, (i + 1) % count) for i in range(ends)])]
    unnamed x27 -> x49, local copies, waits for them, and re-layouts: 4.11 us -> 8.55 us
    all_to_all x1 -> x0, starting transfers between devices: 4.37 us -> none  [sent_to_all(): lax.all_to_all(jnp.broadcast_to(value[None], (count, *value.shape)), axis...]
    reduce_sum x2, other arithmetic: 3.18 us -> 0.16 us  [filter_norm(): jnp.mean(centred * centred, axis=1, keepdims=True) + LN_EPS]
  transfers between devices with their start and end apart: 5 -> 4, of which waited for: 3 -> 2; matrix products, arithmetic and copies ran while one was open for 1% -> 10% of each run, Pallas kernels for 0% -> 0%
where the time goes in v1:
time: 74.2 us; the launch traced here: 73.4 us
  blocking collectives  20.9 us (28%)
  starting transfers between devices  19.1 us (26%)
  local copies, waits for them, and re-layouts  13.3 us (18%)
  waiting for transfers between devices  9.49 us (13%)
  matrix products  8.36 us (11%)
  other arithmetic  1.84 us (2%)
    all_to_all x4, blocking collectives, sent_to_all(): lax.all_to_all(jnp.broadcast_to(value[None], (count, *value.shape)), axis...  20.9 us
    ppermute x2, starting transfers between devices, with_halo(): lax.ppermute(head, axis, [((i + 1) % count, i) for i in range(ends)])  15.3 us
    ppermute x2, waiting for transfers between devices, with_halo(): lax.ppermute(tail, axis, [(i, (i + 1) % count) for i in range(ends)])  9.48 us
    unnamed x49, local copies, waits for them, and re-layouts  8.55 us
    ppermute x2, starting transfers between devices, with_halo(): lax.ppermute(tail, axis, [(i, (i + 1) % count) for i in range(ends)])  3.84 us
    dot_general x6, matrix products, filter_norm(): jnp.dot(padded, forward[:window], preferred_element_type=jnp.float32)  3.59 us
  transfers between devices with their start and end apart: 4, of which 2 were waited for; matrix products, arithmetic and copies ran while one was open for 10% of the time, Pallas kernels for 0%

profile of v1, /device:TPU:385, one launch (start us, length us, event | category | flops | bytes accessed | tf_op | source)
XLA Modules:
  0.0 73.4 jit_solution(15953420851458914314)
XLA Ops:
  0.0 1.1 %broadcast_in_dim.8 = bf16[2,512,512]{2,1,0:T(8,128)(2,1)S(1)} broadcast(bf16[512,512]{1,0:T(8,128)(2,1)} %param.12), dimensions={1,2} | broadcast | bytes 1572864 | tf_op jit(solution)/shard_map/broadcast_in_dim | solution.py:23
  1.1 4.9 %all_to_all.20 = bf16[2,512,512]{2,1,0:T(8,128)(2,1)S(1)} all-to-all(bf16[2,512,512]{2,1,0:T(8,128)(2,1)S(1)} %broadcast_in_dim.8), channel_id=1, replica_groups=mesh['sp'=256,'tp'=2] {'tp'}, dimensions={0} | all-to-all | bytes 2097152 | tf_op jit(solution)/shard_map/all_to_all | solution.py:22
  7.0 0.9 %copy-done.17 = bf16[2,256,1024]{2,1,0:T(8,128)(2,1)S(1)} copy-done((bf16[2,256,1024]{2,1,0:T(8,128)(2,1)S(1)}, bf16[2,256,1024]{2,1,0:T(8,128)(2,1)}, u32[]{:S(2)}) %copy-start.17) | copy-done | bytes 1048600
  8.4 0.7 %copy-done.19 = bf16[2,256,1024]{2,1,0:T(8,128)(2,1)S(1)} copy-done((bf16[2,256,1024]{2,1,0:T(8,128)(2,1)S(1)}, bf16[2,256,1024]{2,1,0:T(8,128)(2,1)}, u32[]{:S(2)}) %copy-start.19) | copy-done | bytes 1048600
  9.7 0.7 fusion.55
  10.4 8.5 %collective-permute-start.1 = (bf16[256,127]{0,1:T(8,128)(2,1)}, bf16[256,127]{0,1:T(8,128)(2,1)}, u32[]{:S(2)}, u32[]{:S(2)}) collective-permute-start(bf16[256,127]{0,1:T(8,128)(2,1)} %get-tuple-element.10), channel_id=1, source_target_pairs={{2,0},{4,2},{6,4},{8,6},{10,8},{12,10},{14,12},{16,14},{18,16},{20... | collective-permute-start | bytes 195080 | tf_op jit(solution)/shard_map/ppermute | solution.py:41
  18.9 1.9 %collective-permute-start = (bf16[256,127]{0,1:T(8,128)(2,1)}, bf16[256,127]{0,1:T(8,128)(2,1)}, u32[]{:S(2)}, u32[]{:S(2)}) collective-permute-start(bf16[256,127]{0,1:T(8,128)(2,1)} %get-tuple-element.9), channel_id=1, source_target_pairs={{0,2},{2,4},{4,6},{6,8},{8,10},{10,12},{12,14},{14,16},{16,18},{18... | collective-permute-start | bytes 195080 | tf_op jit(solution)/shard_map/ppermute | solution.py:39
  22.5 0.8 %copy.35 = bf16[1,256,255]{2,1,0:T(8,128)(2,1)} copy(bf16[1,256,255]{1,0,2:T(2,128)(2,1)S(1)} %get-tuple-element.12) | data formatting | bytes 261120
  23.6 0.6 copy-done.10
  24.5 0.6 fusion.57
  25.1 2.1 %copy.25 = bf16[512,512]{0,1:T(8,128)(2,1)} copy(bf16[512,512]{1,0:T(8,128)(2,1)} %param.12) | data formatting | bytes 1048576 | tf_op args[0]
  27.2 1.1 %fusion.60 = f32[256,768]{1,0:T(8,128)S(1)} fusion(bf16[256,127]{0,1:T(8,128)(2,1)} %collective-permute-done.1, bf16[127,768]{1,0:T(8,128)(2,1)S(1)} %copy-done.8), kind=kOutput, calls=%fused_computation.98 | convolution fusion | flops 49938432 | bytes 1046528 | tf_op jit(solution)/shard_map/dot_general | solution.py:77
  28.3 1.3 %collective-permute-done = bf16[256,127]{0,1:T(8,128)(2,1)} collective-permute-done((bf16[256,127]{0,1:T(8,128)(2,1)}, bf16[256,127]{0,1:T(8,128)(2,1)}, u32[]{:S(2)}, u32[]{:S(2)}) %collective-permute-start) | collective-permute-done | bytes 65056 | tf_op jit(solution)/shard_map/ppermute | solution.py:39
  29.6 1.1 %fusion.13 = f32[256,768]{1,0:T(8,128)S(1)} fusion(f32[256,768]{1,0:T(8,128)S(1)} %fusion.60, f32[256,768]{1,0:T(8,128)S(1)} %fusion.59, bf16[256,127]{0,1:T(8,128)(2,1)} %collective-permute-done, bf16[127,768]{1,0:T(8,128)(2,1)S(1)} %copy-done.6), kind=kOutput, calls=%fused_computation.23 | convolution fusion | flops 50331648 | bytes 2619392 | tf_op jit(solution)/shard_map/dot_general | solution.py:77
  31.1 0.7 copy-done.2
  32.8 5.7 %all_to_all.21 = bf16[2,256,512]{2,1,0:T(8,128)(2,1)S(1)} all-to-all(bf16[2,256,512]{2,1,0:T(8,128)(2,1)S(1)} %broadcast_in_dim.9), channel_id=1, replica_groups=mesh['sp'=256,'tp'=2] {'tp'}, dimensions={0} | all-to-all | bytes 1048576 | tf_op jit(solution)/shard_map/all_to_all | solution.py:22
  39.3 4.6 %all_to_all.22 = bf16[2,512,512]{2,1,0:T(8,128)(2,1)S(1)} all-to-all(bf16[2,512,512]{2,1,0:T(8,128)(2,1)S(1)} %broadcast_in_dim.10), channel_id=1, replica_groups=mesh['sp'=256,'tp'=2] {'tp'}, dimensions={0} | all-to-all | bytes 2097152 | tf_op jit(solution)/shard_map/all_to_all | solution.py:22
  44.5 0.9 %copy-done.18 = bf16[2,256,1024]{2,1,0:T(8,128)(2,1)S(1)} copy-done((bf16[2,256,1024]{2,1,0:T(8,128)(2,1)S(1)}, bf16[2,256,1024]{2,1,0:T(8,128)(2,1)}, u32[]{:S(2)}) %copy-start.18) | copy-done | bytes 1048600
  45.9 0.7 %copy-done.20 = bf16[2,256,1024]{2,1,0:T(8,128)(2,1)S(1)} copy-done((bf16[2,256,1024]{2,1,0:T(8,128)(2,1)S(1)}, bf16[2,256,1024]{2,1,0:T(8,128)(2,1)}, u32[]{:S(2)}) %copy-start.20) | copy-done | bytes 1048600
  47.2 6.8 %collective-permute-start.3 = (bf16[256,127]{0,1:T(8,128)(2,1)S(1)}, bf16[256,127]{0,1:T(8,128)(2,1)S(1)}, u32[]{:S(2)}, u32[]{:S(2)}) collective-permute-start(bf16[256,127]{0,1:T(8,128)(2,1)S(1)} %get-tuple-element.8), channel_id=1, source_target_pairs={{2,0},{4,2},{6,4},{8,6},{10,8},{12,10},{14,12},{16,14},{18,16},{20... | collective-permute-start | bytes 195080 | tf_op jit(solution)/shard_map/ppermute | solution.py:41
  54.4 1.9 %collective-permute-start.2 = (bf16[256,127]{0,1:T(8,128)(2,1)S(1)}, bf16[256,127]{0,1:T(8,128)(2,1)S(1)}, u32[]{:S(2)}, u32[]{:S(2)}) collective-permute-start(bf16[256,127]{0,1:T(8,128)(2,1)S(1)} %get-tuple-element.7), channel_id=1, source_target_pairs={{0,2},{2,4},{4,6},{6,8},{8,10},{10,12},{12,14},{14,16},{16,18},{18... | collective-permute-start | bytes 195080 | tf_op jit(solution)/shard_map/ppermute | solution.py:39
  56.6 8.2 %collective-permute-done.2 = bf16[256,127]{0,1:T(8,128)(2,1)S(1)} collective-permute-done((bf16[256,127]{0,1:T(8,128)(2,1)S(1)}, bf16[256,127]{0,1:T(8,128)(2,1)S(1)}, u32[]{:S(2)}, u32[]{:S(2)}) %collective-permute-start.2) | collective-permute-done | bytes 65056 | tf_op jit(solution)/shard_map/ppermute | solution.py:39
  66.2 5.7 %all_to_all.23 = bf16[2,256,512]{2,1,0:T(8,128)(2,1)S(1)} all-to-all(bf16[2,256,512]{2,1,0:T(8,128)(2,1)S(1)} %broadcast_in_dim.11), channel_id=1, replica_groups=mesh['sp'=256,'tp'=2] {'tp'}, dimensions={0} | all-to-all | bytes 1048576 | tf_op jit(solution)/shard_map/all_to_all | solution.py:22
  72.4 1.0 %copy.31 = bf16[512,512]{1,0:T(8,128)(2,1)} copy(bf16[512,512]{0,1:T(8,128)(2,1)S(1)} %fusion.9) | data formatting | bytes 1048576 | tf_op jit(solution)/shard_map/convert_element_type | solution.py:107
  (83 shorter events, 10.3 us)
Async XLA Ops:
  6.0 0.7 copy-start.12
  6.7 1.2 %copy-start.17 = (bf16[2,256,1024]{2,1,0:T(8,128)(2,1)S(1)}, bf16[2,256,1024]{2,1,0:T(8,128)(2,1)}, u32[]{:S(2)}) copy-start(bf16[2,256,1024]{2,1,0:T(8,128)(2,1)} %param.14) | copy-start | bytes 3145732
  8.0 1.2 %copy-start.19 = (bf16[2,256,1024]{2,1,0:T(8,128)(2,1)S(1)}, bf16[2,256,1024]{2,1,0:T(8,128)(2,1)}, u32[]{:S(2)}) copy-start(bf16[2,256,1024]{2,1,0:T(8,128)(2,1)} %param.15) | copy-start | bytes 3145732
  9.2 11.6 %copy-start = (bf16[512,768]{1,0:T(8,128)(2,1)S(1)}, bf16[512,768]{1,0:T(8,128)(2,1)}, u32[]{:S(2)}) copy-start(bf16[512,768]{1,0:T(8,128)(2,1)} %constant.34) | copy-start | bytes 2359300
  9.7 11.5 %copy-start.5 = (bf16[2,256,255]{1,0,2:T(2,128)(2,1)S(1)}, bf16[2,256,255]{1,0,2:T(2,128)(2,1)}, u32[]{:S(2)}) copy-start(bf16[2,256,255]{1,0,2:T(2,128)(2,1)} %param.16) | copy-start | bytes 783364
  10.4 16.8 %collective-permute-start.1 = (bf16[256,127]{0,1:T(8,128)(2,1)}, bf16[256,127]{0,1:T(8,128)(2,1)}, u32[]{:S(2)}, u32[]{:S(2)}) collective-permute-start(bf16[256,127]{0,1:T(8,128)(2,1)} %get-tuple-element.10), channel_id=1, source_target_pairs={{2,0},{4,2},{6,4},{8,6},{10,8},{12,10},{14,12},{16,14},{18,16},{20... | collective-permute-start | bytes 195080 | tf_op jit(solution)/shard_map/ppermute | solution.py:41
  18.9 10.8 %collective-permute-start = (bf16[256,127]{0,1:T(8,128)(2,1)}, bf16[256,127]{0,1:T(8,128)(2,1)}, u32[]{:S(2)}, u32[]{:S(2)}) collective-permute-start(bf16[256,127]{0,1:T(8,128)(2,1)} %get-tuple-element.9), channel_id=1, source_target_pairs={{0,2},{2,4},{4,6},{6,8},{8,10},{10,12},{12,14},{14,16},{16,18},{18... | collective-permute-start | bytes 195080 | tf_op jit(solution)/shard_map/ppermute | solution.py:39
  21.2 2.1 %copy-start.1 = (bf16[255,768]{1,0:T(8,128)(2,1)S(1)}, bf16[255,768]{1,0:T(8,128)(2,1)}, u32[]{:S(2)}) copy-start(bf16[255,768]{1,0:T(8,128)(2,1)} %constant.30) | copy-start | bytes 1175044
  23.3 0.9 %copy-start.10 = (bf16[1,256,255]{2,1,0:T(8,128)(2,1)S(1)}, bf16[1,256,255]{2,1,0:T(8,128)(2,1)}, u32[]{:S(2)}) copy-start(bf16[1,256,255]{2,1,0:T(8,128)(2,1)} %copy.35) | copy-start | bytes 391684
  23.3 1.2 %copy-start.16 = (f32[2,256]{1,0:T(2,128)S(1)}, f32[2,256]{1,0:T(2,128)}, u32[]{:S(2)}) copy-start(f32[2,256]{1,0:T(2,128)} %param.17) | copy-start | bytes 6148
  24.5 2.7 %copy-start.8 = (bf16[127,768]{1,0:T(8,128)(2,1)S(1)}, bf16[127,768]{1,0:T(8,128)(2,1)}, u32[]{:S(2)}) copy-start(bf16[127,768]{1,0:T(8,128)(2,1)} %constant.35) | copy-start | bytes 585220
  25.1 4.5 %copy-start.6 = (bf16[127,768]{1,0:T(8,128)(2,1)S(1)}, bf16[127,768]{1,0:T(8,128)(2,1)}, u32[]{:S(2)}) copy-start(bf16[127,768]{1,0:T(8,128)(2,1)} %constant.33) | copy-start | bytes 585220
  28.3 2.5 %copy-start.3 = (bf16[384,512]{1,0:T(8,128)(2,1)S(1)}, bf16[384,512]{1,0:T(8,128)(2,1)}, u32[]{:S(2)}) copy-start(bf16[384,512]{1,0:T(8,128)(2,1)} %constant.31) | copy-start | bytes 1179652
  30.8 1.0 %copy-start.2 = (bf16[384,512]{1,0:T(8,128)(2,1)S(1)}, bf16[384,512]{1,0:T(8,128)(2,1)}, u32[]{:S(2)}) copy-start(bf16[384,512]{1,0:T(8,128)(2,1)} %constant.32) | copy-start | bytes 1179652
  32.7 5.8 %copy-start.11 = (bf16[512,512]{0,1:T(8,128)(2,1)S(1)}, bf16[512,512]{0,1:T(8,128)(2,1)}, u32[]{:S(2)}) copy-start(bf16[512,512]{0,1:T(8,128)(2,1)} %copy.25) | copy-start | bytes 1572868
  32.7 5.8 %copy-start.21 = (bf16[2,512,512]{2,1,0:T(8,128)(2,1)S(1)}, bf16[2,512,512]{2,1,0:T(8,128)(2,1)}, u32[]{:S(2)}) copy-start(bf16[2,512,512]{2,1,0:T(8,128)(2,1)} %param.19) | copy-start | bytes 3145732
  44.2 1.2 %copy-start.18 = (bf16[2,256,1024]{2,1,0:T(8,128)(2,1)S(1)}, bf16[2,256,1024]{2,1,0:T(8,128)(2,1)}, u32[]{:S(2)}) copy-start(bf16[2,256,1024]{2,1,0:T(8,128)(2,1)} %param.14) | copy-start | bytes 3145732
  45.4 1.2 %copy-start.20 = (bf16[2,256,1024]{2,1,0:T(8,128)(2,1)S(1)}, bf16[2,256,1024]{2,1,0:T(8,128)(2,1)}, u32[]{:S(2)}) copy-start(bf16[2,256,1024]{2,1,0:T(8,128)(2,1)} %param.15) | copy-start | bytes 3145732
  47.1 9.2 %copy-start.9 = (bf16[127,768]{1,0:T(8,128)(2,1)S(1)}, bf16[127,768]{1,0:T(8,128)(2,1)}, u32[]{:S(2)}) copy-start(bf16[127,768]{1,0:T(8,128)(2,1)} %constant.35) | copy-start | bytes 585220
  47.2 17.7 %copy-start.7 = (bf16[127,768]{1,0:T(8,128)(2,1)S(1)}, bf16[127,768]{1,0:T(8,128)(2,1)}, u32[]{:S(2)}) copy-start(bf16[127,768]{1,0:T(8,128)(2,1)} %constant.33) | copy-start | bytes 585220
  47.2 9.1 %collective-permute-start.3 = (bf16[256,127]{0,1:T(8,128)(2,1)S(1)}, bf16[256,127]{0,1:T(8,128)(2,1)S(1)}, u32[]{:S(2)}, u32[]{:S(2)}) collective-permute-start(bf16[256,127]{0,1:T(8,128)(2,1)S(1)} %get-tuple-element.8), channel_id=1, source_target_pairs={{2,0},{4,2},{6,4},{8,6},{10,8},{12,10},{14,12},{16,14},{18,16},{20... | collective-permute-start | bytes 195080 | tf_op jit(solution)/shard_map/ppermute | solution.py:41
  54.4 10.4 %collective-permute-start.2 = (bf16[256,127]{0,1:T(8,128)(2,1)S(1)}, bf16[256,127]{0,1:T(8,128)(2,1)S(1)}, u32[]{:S(2)}, u32[]{:S(2)}) collective-permute-start(bf16[256,127]{0,1:T(8,128)(2,1)S(1)} %get-tuple-element.7), channel_id=1, source_target_pairs={{0,2},{2,4},{4,6},{6,8},{8,10},{10,12},{12,14},{14,16},{16,18},{18... | collective-permute-start | bytes 195080 | tf_op jit(solution)/shard_map/ppermute | solution.py:39
  56.6 8.5 %copy-start.4 = (bf16[384,512]{1,0:T(8,128)(2,1)S(1)}, bf16[384,512]{1,0:T(8,128)(2,1)}, u32[]{:S(2)}) copy-start(bf16[384,512]{1,0:T(8,128)(2,1)} %constant.31) | copy-start | bytes 1179652
  66.2 5.8 %copy-start.22 = (bf16[2,512,512]{2,1,0:T(8,128)(2,1)S(1)}, bf16[2,512,512]{2,1,0:T(8,128)(2,1)}, u32[]{:S(2)}) copy-start(bf16[2,512,512]{2,1,0:T(8,128)(2,1)} %param.19) | copy-start | bytes 3145732
  (3 other events, 2.0 us)

commit v2 on v0

v2 whole, which is shorter than its diff:
```python
import functools

import jax
import jax.numpy as jnp
import numpy as np
from jax import lax
from jax.experimental import pallas as pl
from jax.experimental.pallas import tpu as pltpu
from jax.sharding import PartitionSpec as P

MESH = pl.DeviceIdType.MESH
BLK = 128
SIZE = 512
HALF = SIZE // 2
RMS_EPS = 1e-06
LN_EPS = 1e-05
F32 = jnp.float32
BF16 = jnp.bfloat16


def tables(taps):
    angle = lambda t: np.asarray(t)[:, None] * ((np.arange(HALF) + 0.5) * (2 * np.pi / SIZE))[None]
    trig = lambda t: np.concatenate([np.cos(angle(t)), np.sin(angle(t))], axis=1)
    blocks = [np.arange(BLK) + BLK * b for b in range(4)]
    reach = (taps - 1) // 2
    forward = [np.concatenate([trig(blocks[b]) for b in order]) for order in ((0, 1, 2, 3), (3, 2, 1, 0))]
    back = [
        np.concatenate([trig(blocks[b] - reach).T for b in order], axis=1) * (2.0 / SIZE)
        for order in ((1, 2), (2, 1))
    ]
    return (
        jnp.asarray(np.stack(forward), BF16),
        jnp.asarray(np.stack(back), BF16),
        jnp.asarray(trig(np.arange(taps)), BF16),
    )


def kernel(
    n_sp,
    x_hbm, ng_hbm, wv_hbm, wg_hbm, taps_hbm, gg_hbm, gs_hbm, wo_hbm, fwd_hbm, back_hbm, ftap_hbm,
    o_ref,
    xin, xs, nrm, wvg, wo, taps, ngv, ggv, gsv, ngb, ggb, gsb, resp, fwd, back, ftap,
    g1, g2, gfar, gpar1, gpar2, act, obuf,
    lsem, ssem, rsem,
):
    sp, c = lax.axis_index("sp"), lax.axis_index("tp")
    p = 1 - c
    outer = sp + 2 * c - 1
    has_left = sp > 0
    has_right = sp < n_sp - 1
    has_outer = jnp.logical_and(outer >= 0, outer < n_sp)
    left_count = jnp.where(has_left, 1, 0)
    right_count = jnp.where(has_right, 1, 0)
    layers = wv_hbm.shape[0]

    barrier = pltpu.get_barrier_semaphore()
    pl.semaphore_signal(barrier, inc=1, device_id=(sp, p), device_id_type=MESH)

    @pl.when(has_outer)
    def _():
        for core in range(2):
            pl.semaphore_signal(barrier, inc=1, device_id=(outer, core), device_id_type=MESH)

    local, count = {}, [0]

    def load(name, src, dst):
        copy = pltpu.make_async_copy(src, dst, lsem.at[count[0]])
        count[0] += 1
        copy.start()
        local.setdefault(name, []).append(copy)

    def loaded(name):
        for copy in local[name]:
            copy.wait()

    for b in range(4):
        load("x", x_hbm.at[:, pl.ds(b * BLK, BLK)], xin.at[b])
    load("ng", ng_hbm, ngv)
    load("gg", gg_hbm, ggv.at[c])
    load("gs", gs_hbm, gsv.at[c])
    load("taps", taps_hbm, taps.at[c])
    load("ftap", ftap_hbm, ftap)

    def load_wvg(l):
        for k in range(2):
            load(f"wvg{l}", wv_hbm.at[l, pl.ds(k * BLK, BLK)], wvg.at[l, c, k, 0])
            load(f"wvg{l}", wg_hbm.at[l, pl.ds(k * BLK, BLK)], wvg.at[l, c, k, 1])

    load_wvg(0)
    load("tables", fwd_hbm.at[c], fwd)
    load("tables", back_hbm.at[c], back)
    load("wo0", wo_hbm.at[0], wo.at[0, c])
    load_wvg(1)
    load("wo1", wo_hbm.at[1], wo.at[1, c])

    sent = []

    def remote(k, src, dst, device):
        return pltpu.make_async_remote_copy(
            src_ref=src, dst_ref=dst, send_sem=ssem.at[k], recv_sem=rsem.at[k],
            device_id=device, device_id_type=MESH,
        )

    def to_partner(k, src, dst):
        copy = remote(k, src, dst, (sp, p))
        copy.start()
        sent.append(copy)

    def from_partner(k, dst):
        remote(k, dst, dst, (sp, p)).wait_recv()

    def column(row):
        return jnp.broadcast_to(row, (BLK, BLK)).T

    def spread_groups(h):
        for l in range(layers):
            for b in range(2):
                lanes = slice(b * BLK, (b + 1) * BLK)
                ggb[l, h, lanes] = column(ggv[h, l : l + 1, lanes])
                gsb[l, h, lanes] = column(gsv[h, l : l + 1, lanes])

    def respond(h):
        for l in range(layers):
            resp[l, h] = jnp.dot(taps[h, l], ftap[...], preferred_element_type=F32)

    loaded("ng")
    for l in range(layers):
        for b in range(ngv.shape[1] // BLK):
            rows = slice(b * BLK, (b + 1) * BLK)
            ngb[l, rows] = column(ngv[l : l + 1, rows])
    loaded("gg")
    loaded("gs")
    loaded("taps")
    loaded("ftap")
    respond(c)
    spread_groups(c)
    loaded("x")

    pl.semaphore_wait(barrier, 1 + left_count + right_count)

    NEAR, FAR, XMID, XINN, WVG, WO, TAPS, GG, GS, PAR1, PAR2, OMID, OINN, SR = 0, 2, 3, 4, 5, 7, 9, 10, 11, 12, 13, 14, 15, 16
    near = (slice(None), pl.ds(0, BLK))

    def near_copy(b, send, device):
        return pltpu.make_async_remote_copy(
            src_ref=xin.at[b], dst_ref=xs.at[(c, *near)], send_sem=ssem.at[send], recv_sem=rsem.at[NEAR + c],
            device_id=device, device_id_type=MESH,
        )

    to_left = near_copy(0, NEAR, (sp - 1, 1))
    to_right = near_copy(3, NEAR + 1, (sp + 1, 0))

    @pl.when(has_left)
    def _():
        to_left.start()

    @pl.when(has_right)
    def _():
        to_right.start()

    mid, inn = pl.ds(BLK, BLK), pl.ds(2 * BLK, BLK)
    to_partner(XINN, xin.at[1 + p], xs.at[c, :, inn])
    to_partner(XMID, xin.at[3 * p], xs.at[c, :, mid])
    loaded("wvg0")
    to_partner(WVG, wvg.at[0, c], wvg.at[0, c])
    to_partner(TAPS, taps.at[c], taps.at[c])
    to_partner(GG, ggv.at[c], ggv.at[c])
    to_partner(GS, gsv.at[c], gsv.at[c])
    loaded("wo0")
    to_partner(WO, wo.at[0, c], wo.at[0, c])

    xs[c, :, BLK : 2 * BLK] = xin[3 * c]
    xs[c, :, 2 * BLK : 3 * BLK] = xin[1 + c]

    def normalize(l, blocks):
        for b in blocks:
            lanes = slice(b * BLK, (b + 1) * BLK)
            rows = xs.shape[1]
            total = jnp.zeros((1, BLK), F32)
            for h in range(2):
                wide = xs[h, :, lanes].astype(F32)
                total = total + jnp.sum(wide * wide, axis=0, keepdims=True)
            inverse = lax.rsqrt(total * (1.0 / (2 * rows)) + RMS_EPS)
            for h in range(2):
                wide = xs[h, :, lanes].astype(F32)
                part = slice(h * rows, (h + 1) * rows)
                nrm[part, lanes] = (wide * inverse * ngb[l, part]).astype(BF16)

    def gate(l, h, lanes, dst, scale=None):
        w = wvg[l, h].reshape(4 * BLK, wvg.shape[-1])
        r = jnp.dot(w, nrm[:, lanes], preferred_element_type=F32)
        for k in range(2):
            value = r[2 * k * BLK : (2 * k + 1) * BLK]
            gating = r[(2 * k + 1) * BLK : (2 * k + 2) * BLK]
            out = value * (0.5 * jnp.tanh(0.5 * gating) + 0.5)
            if scale is not None:
                out = out * scale
            dst[h, k * BLK : (k + 1) * BLK, lanes] = out.astype(BF16)

    def filter_norm(l, window, outputs, lanes):
        n = outputs.stop - outputs.start
        for h in range(2):
            w = window(h)
            g = jnp.dot(w, fwd[: w.shape[1]], preferred_element_type=F32)
            gr, gi = g[:, :HALF], g[:, HALF:]
            hr, hi = resp[l, h, :, :HALF], resp[l, h, :, HALF:]
            y = jnp.concatenate([(gr * hr + gi * hi).astype(BF16), (gi * hr - gr * hi).astype(BF16)], axis=1)
            filtered = jnp.dot(y, back[:, outputs], preferred_element_type=F32)
            for k in range(2):
                rows = slice(k * BLK, (k + 1) * BLK)
                f = filtered[rows]
                centred = f - jnp.sum(f, axis=0, keepdims=True) * (1.0 / BLK)
                variance = jnp.sum(centred * centred, axis=0, keepdims=True) * (1.0 / BLK)
                gain, shift = ggb[l, h, rows], gsb[l, h, rows]
                if n > BLK:
                    gain = jnp.concatenate([gain] * (n // BLK), axis=1)
                    shift = jnp.concatenate([shift] * (n // BLK), axis=1)
                s = centred * lax.rsqrt(variance + LN_EPS) * gain + shift
                act[h * 2 * BLK + k * BLK : h * 2 * BLK + (k + 1) * BLK, lanes] = (
                    0.5 * s * (1.0 + jnp.tanh(0.5 * s))
                ).astype(BF16)

    def project_out(l, h, lanes):
        return xs[h, :, lanes].astype(F32) + jnp.dot(wo[l, h], act[:, lanes], preferred_element_type=F32)

    def advance(l, lanes):
        for h in range(2):
            xs[h, :, lanes] = project_out(l, h, lanes).astype(BF16)

    own, outside = slice(BLK, 3 * BLK), slice(0, BLK)

    from_partner(XINN, xs.at[p, :, inn])
    from_partner(XMID, xs.at[p, :, mid])
    normalize(0, (1, 2))
    gate(0, c, own, g1)
    from_partner(WVG, wvg.at[0, p])
    gate(0, p, own, g1)
    inner1 = g1.at[:, :, inn]
    to_outer = remote(FAR, inner1, gfar, (outer, p))

    @pl.when(has_outer)
    def _():
        to_outer.start()

    to_partner(PAR1, inner1, gpar1)
    loaded("wvg1")
    to_partner(WVG + 1, wvg.at[1, c], wvg.at[1, c])
    loaded("wo1")
    to_partner(WO + 1, wo.at[1, c], wo.at[1, c])

    from_partner(TAPS, taps.at[p])
    respond(p)
    from_partner(GG, ggv.at[p])
    from_partner(GS, gsv.at[p])
    spread_groups(p)
    loaded("tables")

    @pl.when(has_outer)
    def _():
        for core in range(2):
            dst = xs.at[(core, *near)]
            pltpu.make_async_remote_copy(
                src_ref=dst, dst_ref=dst, send_sem=ssem.at[NEAR], recv_sem=rsem.at[NEAR + core],
                device_id=(outer, core), device_id_type=MESH,
            ).wait_recv()

    @pl.when(jnp.logical_not(has_outer))
    def _():
        xs[:, :, outside] = jnp.zeros((2, xs.shape[1], BLK), BF16)
        gfar[...] = jnp.zeros_like(gfar)

    normalize(0, (0,))
    for h in range(2):
        gate(0, h, outside, g1)

    from_partner(PAR1, gpar1)
    filter_norm(0, lambda h: jnp.concatenate([g1[h], gpar1[h]], axis=1), slice(0, 2 * BLK), own)
    from_partner(WO, wo.at[0, p])
    advance(0, own)

    normalize(1, (1, 2))
    gate(1, c, own, g2)
    from_partner(WVG + 1, wvg.at[1, p])
    gate(1, p, own, g2)
    to_partner(PAR2, g2.at[:, :, inn], gpar2)

    @pl.when(has_outer)
    def _():
        remote(FAR, gfar, gfar, (outer, p)).wait_recv()

    filter_norm(0, lambda h: jnp.concatenate([gfar[h], g1[h, :, : 2 * BLK]], axis=1), slice(0, BLK), outside)
    advance(0, outside)

    normalize(1, (0,))
    exists = jnp.where(has_outer, 1.0, 0.0)
    for h in range(2):
        gate(1, h, outside, g2, exists)
    from_partner(PAR2, gpar2)
    filter_norm(1, lambda h: jnp.concatenate([g2[h], gpar2[h]], axis=1), slice(0, 2 * BLK), own)
    from_partner(WO + 1, wo.at[1, p])

    obuf[...] = project_out(1, p, own).astype(BF16)
    columns = lambda core: (
        pl.ds(pl.multiple_of(core * 3 * BLK, BLK), BLK),
        pl.ds(pl.multiple_of((1 + core) * BLK, BLK), BLK),
    )
    for k, (lane, b) in enumerate(zip(columns(c), range(2))):
        to_partner(OMID + k, obuf.at[:, pl.ds(b * BLK, BLK)], o_ref.at[:, lane])
    kept = project_out(1, c, own).astype(BF16)
    for lane, b in zip(columns(c), range(2)):
        o_ref[:, lane] = kept[:, b * BLK : (b + 1) * BLK]
    for k, lane in enumerate(columns(p)):
        from_partner(OMID + k, o_ref.at[:, lane])

    for copy in sent:
        copy.wait_send()

    @pl.when(has_left)
    def _():
        to_left.wait_send()

    @pl.when(has_right)
    def _():
        to_right.wait_send()

    @pl.when(has_outer)
    def _():
        to_outer.wait_send()


def solution(mesh):
    n_sp = mesh.shape["sp"]

    def body(stream, norm_gain, w_value, w_gate, conv_taps, group_gain, group_shift, w_out):
        layers, features = norm_gain.shape
        half_features, tokens = stream.shape
        channels = w_value.shape[1]
        taps = conv_taps.shape[2]
        any_spec = pl.BlockSpec(memory_space=pl.ANY)
        vmem = pltpu.VMEM
        return pl.pallas_call(
            functools.partial(kernel, n_sp),
            out_shape=jax.ShapeDtypeStruct(stream.shape, stream.dtype),
            in_specs=[any_spec] * 11,
            out_specs=pl.BlockSpec(memory_space=pltpu.VMEM),
            scratch_shapes=[
                vmem((4, half_features, BLK), BF16),
                vmem((2, half_features, 3 * BLK), BF16),
                vmem((features, 3 * BLK), BF16),
                vmem((layers, 2, 2, 2, BLK, features), BF16),
                vmem((layers, 2, half_features, 2 * channels), BF16),
                vmem((2, layers, channels, taps), BF16),
                vmem((layers, features), F32),
                vmem((2, layers, channels), F32),
                vmem((2, layers, channels), F32),
                vmem((layers, features, BLK), F32),
                vmem((layers, 2, channels, BLK), F32),
                vmem((layers, 2, channels, BLK), F32),
                vmem((layers, 2, channels, SIZE), F32),
                vmem((SIZE, SIZE), BF16),
                vmem((SIZE, 2 * BLK), BF16),
                vmem((taps, SIZE), BF16),
                vmem((2, channels, 3 * BLK), BF16),
                vmem((2, channels, 3 * BLK), BF16),
                vmem((2, channels, BLK), BF16),
                vmem((2, channels, BLK), BF16),
                vmem((2, channels, BLK), BF16),
                vmem((2 * channels, 3 * BLK), BF16),
                vmem((half_features, 2 * BLK), BF16),
                pltpu.SemaphoreType.DMA((21,)),
                pltpu.SemaphoreType.DMA((16,)),
                pltpu.SemaphoreType.DMA((16,)),
            ],
            compiler_params=pltpu.CompilerParams(
                collective_id=0, has_side_effects=True, vmem_limit_bytes=60 * 1024 * 1024
            ),
        )(stream, norm_gain, w_value, w_gate, conv_taps, group_gain, group_shift, w_out, *tables(taps))

    placed = (
        P("tp", "sp"),
        P(),
        P(None, "tp", None),
        P(None, "tp", None),
        P(None, "tp", None),
        P(None, "tp"),
        P(None, "tp"),
        P(None, "tp", None),
    )
    return jax.shard_map(body, mesh=mesh, in_specs=placed, out_specs=P("tp", "sp"), check_vma=False)
```

time: 113 us -> 27.8 us (0.25)
  matrix products: 43.1 us -> 0 us
  Pallas kernels: 0 us -> 24 us
  starting transfers between devices: 20.2 us -> 0 us
  waiting for transfers between devices: 15.9 us -> 0 us
  blocking collectives: 15.7 us -> 0 us
  local copies, waits for them, and re-layouts: 10.2 us -> 3.69 us
  other arithmetic: 6.41 us -> 0 us
    conv_general_dilated x2 -> x0, matrix products: 40.1 us -> none  [filter_norm(): lax.conv_general_dilated(padded[None], taps[:, None, :], (1,), [(0, 0)],...]
    pallas_call x0 -> x1, Pallas kernels: none -> 24 us  [body(): pl.pallas_call(functools.partial(kernel, n_sp), out_shape=jax.ShapeDtypeS...]
    ppermute x4 -> x0, starting transfers between devices: 15.8 us -> none  [the longest x2 10.5 us: with_halo(): lax.ppermute(head, axis, [((i + 1) % count, i) for i in range(ends)])]
    all_to_all x3 -> x0, blocking collectives: 15.7 us -> none  [sent_to_all(): lax.all_to_all(jnp.broadcast_to(value[None], (count, *value.shape)), axis...]
    ppermute x4 -> x0, waiting for transfers between devices: 14.2 us -> none  [the longest x2 14.2 us: with_halo(): lax.ppermute(tail, axis, [(i, (i + 1) % count) for i in range(ends)])]
    reduce_sum x6 -> x0, other arithmetic: 4.96 us -> none  [the longest x2 3.18 us: filter_norm(): jnp.mean(centred * centred, axis=1, keepdims=True) + LN_EPS]
    all_to_all x1 -> x0, starting transfers between devices: 4.37 us -> none  [sent_to_all(): lax.all_to_all(jnp.broadcast_to(value[None], (count, *value.shape)), axis...]
    dot_general x6 -> x0, matrix products: 2.94 us -> none  [the longest x2 1.01 us: make_gated(): jnp.dot(gate_weight, normed, preferred_element_type=jnp.float32)]
  transfers between devices with their start and end apart: 5 -> 0, of which waited for: 3 -> 0; matrix products, arithmetic and copies ran while one was open for 1% -> 0% of each run, Pallas kernels for 0% -> 0%
where the time goes in v2:
time: 27.8 us; the launch traced here: 27.7 us
  Pallas kernels  24 us (86%)
  local copies, waits for them, and re-layouts  3.69 us (13%)
    pallas_call x1, Pallas kernels, body(): pl.pallas_call(functools.partial(kernel, n_sp), out_shape=jax.ShapeDtypeS...  24 us
    unnamed x2, local copies, waits for them, and re-layouts  3.69 us

profile of v2, /device:TPU:385, one launch (start us, length us, event | category | flops | bytes accessed | tf_op | source)
XLA Modules:
  0.0 27.7 jit_solution(4584118328217016749)
XLA Ops:
  0.0 1.8 %copy.12.taps_hbm = bf16[2,256,255]{2,1,0:T(8,128)(2,1)} copy(bf16[2,256,255]{1,0,2:T(2,128)(2,1)} %param.15) | data formatting | bytes 522240 | tf_op args[4]
  1.8 24.0 %shard_map.109 = bf16[512,512]{1,0:T(8,128)(2,1)} custom-call(bf16[512,512]{1,0:T(8,128)(2,1)} %x_hbm.1, f32[2,1024]{1,0:T(2,128)} %ng_hbm.1, bf16[2,256,1024]{2,1,0:T(8,128)(2,1)} %wv_hbm.1, bf16[2,256,1024]{2,1,0:T(8,128)(2,1)} %wg_hbm.1, bf16[2,256,255]{2,1,0:T(8,128)(2,1)} %copy.12.taps_hbm, f32[2,256]{1,0:T(2,128)} %gg_hbm.1, f32[2,256]{1,0:T(2,128)} %gs_hbm.1, ...), custom_call_target="tpu_custom_call" | custom-call | tf_op jit(solution)/shard_map/pallas_call | solution.py:341
  25.8 1.9 %copy.14 = bf16[512,512]{1,0:T(8,128)(2,1)} copy(bf16[512,512]{1,0:T(8,128)(2,1)} %shard_map.109) | data formatting | bytes 1048576

commit v3 on v2

v3 whole, which is shorter than its diff:
```python
import functools

import jax
import jax.numpy as jnp
import numpy as np
from jax import lax
from jax.experimental import pallas as pl
from jax.experimental.pallas import tpu as pltpu
from jax.sharding import PartitionSpec as P

MESH = pl.DeviceIdType.MESH
BLK = 128
SIZE = 512
HALF = SIZE // 2
RMS_EPS = 1e-06
LN_EPS = 1e-05
F32 = jnp.float32
BF16 = jnp.bfloat16


def tables(taps):
    angle = lambda t: np.asarray(t)[:, None] * ((np.arange(HALF) + 0.5) * (2 * np.pi / SIZE))[None]
    trig = lambda t: np.concatenate([np.cos(angle(t)), np.sin(angle(t))], axis=1)
    blocks = [np.arange(BLK) + BLK * b for b in range(4)]
    reach = (taps - 1) // 2
    forward = [np.concatenate([trig(blocks[b]) for b in order]) for order in ((0, 1, 2, 3), (3, 2, 1, 0))]
    back = [
        np.concatenate([trig(blocks[b] - reach).T for b in order], axis=1) * (2.0 / SIZE)
        for order in ((1, 2), (2, 1))
    ]
    mixed = np.zeros((2, 2 * BLK, 2, 2 * HALF))
    for layer in range(2):
        mixed[layer, :taps, layer] = trig(np.arange(taps))
    return (
        jnp.asarray(np.stack(forward), BF16),
        jnp.asarray(np.stack(back), BF16),
        jnp.asarray(mixed.reshape(2, 4 * BLK, SIZE), BF16),
    )


def kernel(
    n_sp,
    x_hbm, ng_hbm, wv_hbm, wg_hbm, taps_hbm, gg_hbm, gs_hbm, wo_hbm, fwd_hbm, back_hbm, ftap_hbm,
    o_ref,
    xin, xs, wraw, wvg, wo, taps, ngv, ggv, gsv, ggb, gsb, resp, fwd, back, ftap,
    g1, g2, gfar, gpar1, gpar2, act, obuf,
    lsem, ssem, rsem, ready,
):
    sp, c = lax.axis_index("sp"), lax.axis_index("tp")
    p = 1 - c
    outer = sp + 2 * c - 1
    has_left = sp > 0
    has_right = sp < n_sp - 1
    has_outer = jnp.logical_and(outer >= 0, outer < n_sp)
    left_count = jnp.where(has_left, 1, 0)
    right_count = jnp.where(has_right, 1, 0)
    layers, features = ng_hbm.shape

    barrier = pltpu.get_barrier_semaphore()
    pl.semaphore_signal(barrier, inc=1, device_id=(sp, p), device_id_type=MESH)

    @pl.when(has_outer)
    def _():
        pl.semaphore_signal(barrier, inc=1, device_id=(outer, 1), device_id_type=MESH)

    local, count = {}, [0]

    def load(name, src, dst):
        copy = pltpu.make_async_copy(src, dst, lsem.at[count[0]])
        count[0] += 1
        copy.start()
        local.setdefault(name, []).append(copy)

    def loaded(*names):
        for name in names:
            for copy in local[name]:
                copy.wait()

    def load_wvg(l):
        for k in range(2):
            load(f"w{l}", wv_hbm.at[l, pl.ds(k * BLK, BLK)], wraw.at[l, k, 0])
            load(f"w{l}", wg_hbm.at[l, pl.ds(k * BLK, BLK)], wraw.at[l, k, 1])

    for b in range(4):
        load("x", x_hbm.at[:, pl.ds(b * BLK, BLK)], xin.at[b])
    load("ng", ng_hbm, ngv)
    load_wvg(0)
    load("groups", gg_hbm, ggv.at[c])
    load("groups", gs_hbm, gsv.at[c])
    load("taps", taps_hbm, taps.at[pl.ds(0, taps_hbm.shape[0])])
    load("taps", ftap_hbm, ftap)
    load("tables", fwd_hbm.at[c], fwd)
    load("tables", back_hbm.at[c], back)
    load("wo0", wo_hbm.at[0], wo.at[0, c])
    load_wvg(1)
    load("wo1", wo_hbm.at[1], wo.at[1, c])

    NEAR, FAR, XMID, XINN, WVG, WO, RESP, GG, GS, PAR1, PAR2, OMID = 0, 2, 3, 4, 5, 7, 9, 11, 12, 13, 14, 15
    sent = []

    def remote(k, src, dst, device):
        return pltpu.make_async_remote_copy(
            src_ref=src, dst_ref=dst, send_sem=ssem.at[k], recv_sem=rsem.at[k],
            device_id=device, device_id_type=MESH,
        )

    def to_partner(k, src, dst):
        copy = remote(k, src, dst, (sp, p))
        copy.start()
        sent.append(copy)

    def from_partner(k, dst):
        remote(k, dst, dst, (sp, p)).wait_recv()

    def scale_weights(l):
        gain = ngv[l : l + 1]
        for k in range(2):
            for half in range(2):
                wvg[l, c, k, half] = (wraw[l, k, half].astype(F32) * gain).astype(BF16)

    def spread_groups(h):
        column = lambda row: jnp.broadcast_to(row * 0.5, (BLK, BLK)).T
        for l in range(layers):
            for b in range(2):
                lanes = slice(b * BLK, (b + 1) * BLK)
                ggb[l, h, lanes] = column(ggv[h, l : l + 1, lanes])
                gsb[l, h, lanes] = column(gsv[h, l : l + 1, lanes])

    loaded("x")

    @pl.when(c == 0)
    def _():
        pl.semaphore_wait(barrier, 1)
        pl.semaphore_signal(ready, inc=1, device_id=(sp, 1), device_id_type=MESH)

    @pl.when(c == 1)
    def _():
        pl.semaphore_wait(ready, 1)

    mid, inn = pl.ds(BLK, BLK), pl.ds(2 * BLK, BLK)
    to_partner(XINN, xin.at[1 + p], xs.at[c, :, inn])
    to_partner(XMID, xin.at[3 * p], xs.at[c, :, mid])
    loaded("ng", "w0")
    scale_weights(0)
    loaded("groups")
    to_partner(GG, ggv.at[c], ggv.at[c])
    to_partner(GS, gsv.at[c], gsv.at[c])
    to_partner(WVG, wvg.at[0, c], wvg.at[0, c])

    @pl.when(c == 1)
    def _():
        pl.semaphore_wait(barrier, 1 + left_count + right_count)
        pl.semaphore_signal(ready, inc=1, device_id=(sp, 0), device_id_type=MESH)

    @pl.when(c == 0)
    def _():
        pl.semaphore_wait(ready, 1)

    near = (slice(None), pl.ds(0, BLK))

    def near_copy(b, send, device):
        return pltpu.make_async_remote_copy(
            src_ref=xin.at[b], dst_ref=xs.at[(c, *near)], send_sem=ssem.at[send], recv_sem=rsem.at[NEAR + c],
            device_id=device, device_id_type=MESH,
        )

    to_left = near_copy(0, NEAR, (sp - 1, 1))
    to_right = near_copy(3, NEAR + 1, (sp + 1, 0))

    @pl.when(has_left)
    def _():
        to_left.start()

    @pl.when(has_right)
    def _():
        to_right.start()

    loaded("taps")
    taps[taps_hbm.shape[0] :] = jnp.zeros((taps.shape[0] - taps_hbm.shape[0], *taps.shape[1:]), BF16)
    rows = taps[...].reshape(layers * taps.shape[0], taps.shape[2])
    for l in range(layers):
        resp[l, c] = lax.dot_general(
            rows, ftap[l], (((0,), (0,)), ((), ())), preferred_element_type=F32
        ).astype(BF16)
    spread_groups(c)
    to_partner(RESP, resp.at[0, c], resp.at[0, c])

    xs[c, :, BLK : 2 * BLK] = xin[3 * c]
    xs[c, :, 2 * BLK : 3 * BLK] = xin[1 + c]

    def half_inverse(lanes):
        total = jnp.zeros((1, lanes.stop - lanes.start), F32)
        for h in range(2):
            wide = xs[h, :, lanes].astype(F32)
            total = total + jnp.sum(wide * wide, axis=0, keepdims=True)
        return 0.5 * lax.rsqrt(total * (1.0 / features) + RMS_EPS)

    def gate(l, halves, lanes, dst, inverse, exists=None):
        x = xs[:, :, lanes].reshape(features, lanes.stop - lanes.start)
        kept = inverse if exists is None else inverse * exists
        for h in halves:
            for k in range(2):
                w = wvg[l, h, k].reshape(2 * BLK, features)
                r = jnp.dot(w, x, preferred_element_type=F32)
                value = r[:BLK] * kept
                out = value * jnp.tanh(r[BLK:] * inverse) + value
                dst[h, k * BLK : (k + 1) * BLK, lanes] = out.astype(BF16)

    def filter_norm(l, window, outputs, lanes):
        n = outputs.stop - outputs.start
        for h in range(2):
            w = window(h)
            g = jnp.dot(w, fwd[: w.shape[1]], preferred_element_type=F32)
            gr, gi = g[:, :HALF], g[:, HALF:]
            hr, hi = resp[l, h, :, :HALF].astype(F32), resp[l, h, :, HALF:].astype(F32)
            y = jnp.concatenate([(gr * hr + gi * hi).astype(BF16), (gi * hr - gr * hi).astype(BF16)], axis=1)
            filtered = jnp.dot(y, back[:, outputs], preferred_element_type=F32)
            for k in range(2):
                part = slice(k * BLK, (k + 1) * BLK)
                f = filtered[part]
                centred = f - jnp.sum(f, axis=0, keepdims=True) * (1.0 / BLK)
                variance = jnp.sum(centred * centred, axis=0, keepdims=True) * (1.0 / BLK)
                gain, shift = ggb[l, h, part], gsb[l, h, part]
                if n > BLK:
                    gain = jnp.concatenate([gain] * (n // BLK), axis=1)
                    shift = jnp.concatenate([shift] * (n // BLK), axis=1)
                s = centred * lax.rsqrt(variance + LN_EPS) * gain + shift
                act[h * 2 * BLK + k * BLK : h * 2 * BLK + (k + 1) * BLK, lanes] = (s * jnp.tanh(s) + s).astype(BF16)

    def project_out(l, h, lanes, dst, dst_lanes):
        for half in range(2):
            part = slice(half * 2 * BLK, (half + 1) * 2 * BLK)
            branch = jnp.dot(wo[l, h, part], act[:, lanes], preferred_element_type=F32)
            dst[part, dst_lanes] = (xs[h, part, lanes].astype(F32) + branch).astype(BF16)

    def advance(l, lanes):
        for h in range(2):
            project_out(l, h, lanes, xs.at[h], lanes)

    own, outside = slice(BLK, 3 * BLK), slice(0, BLK)

    from_partner(XINN, xs.at[p, :, inn])
    from_partner(XMID, xs.at[p, :, mid])
    inverse = half_inverse(own)
    gate(0, (c,), own, g1, inverse)
    from_partner(GG, ggv.at[p])
    from_partner(GS, gsv.at[p])
    spread_groups(p)
    from_partner(WVG, wvg.at[0, p])
    gate(0, (p,), own, g1, inverse)
    inner1 = g1.at[:, :, inn]
    to_outer = remote(FAR, inner1, gfar, (outer, p))

    @pl.when(has_outer)
    def _():
        to_outer.start()

    to_partner(PAR1, inner1, gpar1)
    loaded("wo0")
    to_partner(WO, wo.at[0, c], wo.at[0, c])
    loaded("w1")
    scale_weights(1)
    to_partner(WVG + 1, wvg.at[1, c], wvg.at[1, c])
    to_partner(RESP + 1, resp.at[1, c], resp.at[1, c])
    loaded("wo1")
    to_partner(WO + 1, wo.at[1, c], wo.at[1, c])
    loaded("tables")

    @pl.when(has_outer)
    def _():
        for core in range(2):
            dst = xs.at[(core, *near)]
            pltpu.make_async_remote_copy(
                src_ref=dst, dst_ref=dst, send_sem=ssem.at[NEAR], recv_sem=rsem.at[NEAR + core],
                device_id=(outer, core), device_id_type=MESH,
            ).wait_recv()

    @pl.when(jnp.logical_not(has_outer))
    def _():
        xs[:, :, outside] = jnp.zeros((2, xs.shape[1], BLK), BF16)
        gfar[...] = jnp.zeros_like(gfar)

    gate(0, (0, 1), outside, g1, half_inverse(outside))

    from_partner(RESP, resp.at[0, p])
    from_partner(PAR1, gpar1)
    filter_norm(0, lambda h: jnp.concatenate([g1[h], gpar1[h]], axis=1), slice(0, 2 * BLK), own)
    from_partner(WO, wo.at[0, p])
    advance(0, own)

    from_partner(WVG + 1, wvg.at[1, p])
    gate(1, (0, 1), own, g2, half_inverse(own))
    to_partner(PAR2, g2.at[:, :, inn], gpar2)

    @pl.when(has_outer)
    def _():
        remote(FAR, gfar, gfar, (outer, p)).wait_recv()

    filter_norm(0, lambda h: jnp.concatenate([gfar[h], g1[h, :, : 2 * BLK]], axis=1), slice(0, BLK), outside)
    advance(0, outside)

    gate(1, (0, 1), outside, g2, half_inverse(outside), jnp.where(has_outer, 1.0, 0.0))
    from_partner(RESP + 1, resp.at[1, p])
    from_partner(PAR2, gpar2)
    filter_norm(1, lambda h: jnp.concatenate([g2[h], gpar2[h]], axis=1), slice(0, 2 * BLK), own)
    from_partner(WO + 1, wo.at[1, p])

    columns = lambda core: (
        pl.ds(pl.multiple_of(core * 3 * BLK, BLK), BLK),
        pl.ds(pl.multiple_of((1 + core) * BLK, BLK), BLK),
    )
    whole = slice(0, 2 * BLK)
    project_out(1, p, own, obuf.at[0], whole)
    for k, lane in enumerate(columns(c)):
        to_partner(OMID + k, obuf.at[0, :, pl.ds(k * BLK, BLK)], o_ref.at[:, lane])
    project_out(1, c, own, obuf.at[1], whole)
    for k, lane in enumerate(columns(c)):
        o_ref[:, lane] = obuf[1, :, k * BLK : (k + 1) * BLK]
    for k, lane in enumerate(columns(p)):
        from_partner(OMID + k, o_ref.at[:, lane])

    for copy in sent:
        copy.wait_send()

    @pl.when(has_left)
    def _():
        to_left.wait_send()

    @pl.when(has_right)
    def _():
        to_right.wait_send()

    @pl.when(has_outer)
    def _():
        to_outer.wait_send()


def write_kernel(src, dst, sem):
    copy = pltpu.make_async_copy(src, dst, sem)
    copy.start()
    copy.wait()


def write_out(value):
    return pl.pallas_call(
        write_kernel,
        out_shape=jax.ShapeDtypeStruct(value.shape, value.dtype),
        in_specs=[pl.BlockSpec(memory_space=pltpu.VMEM)],
        out_specs=pl.BlockSpec(memory_space=pl.ANY),
        scratch_shapes=[pltpu.SemaphoreType.DMA],
        compiler_params=pltpu.CompilerParams(vmem_limit_bytes=1024 * 1024),
    )(pltpu.with_memory_space_constraint(value, pltpu.VMEM))


def solution(mesh):
    n_sp = mesh.shape["sp"]

    def body(stream, norm_gain, w_value, w_gate, conv_taps, group_gain, group_shift, w_out):
        layers, features = norm_gain.shape
        half_features, tokens = stream.shape
        channels = w_value.shape[1]
        taps = conv_taps.shape[2]
        any_spec = pl.BlockSpec(memory_space=pl.ANY)
        vmem = pltpu.VMEM
        result = pl.pallas_call(
            functools.partial(kernel, n_sp),
            out_shape=pltpu.VMEM(stream.shape, stream.dtype),
            in_specs=[any_spec] * 11,
            out_specs=pl.BlockSpec(memory_space=pltpu.VMEM),
            scratch_shapes=[
                vmem((4, half_features, BLK), BF16),
                vmem((2, half_features, 3 * BLK), BF16),
                vmem((layers, 2, 2, BLK, features), BF16),
                vmem((layers, 2, 2, 2, BLK, features), BF16),
                vmem((layers, 2, half_features, 2 * channels), BF16),
                vmem((2 * BLK, layers, channels), BF16),
                vmem((layers, features), F32),
                vmem((2, layers, channels), F32),
                vmem((2, layers, channels), F32),
                vmem((layers, 2, channels, BLK), F32),
                vmem((layers, 2, channels, BLK), F32),
                vmem((layers, 2, channels, SIZE), BF16),
                vmem((SIZE, SIZE), BF16),
                vmem((SIZE, 2 * BLK), BF16),
                vmem((layers, SIZE, SIZE), BF16),
                vmem((2, channels, 3 * BLK), BF16),
                vmem((2, channels, 3 * BLK), BF16),
                vmem((2, channels, BLK), BF16),
                vmem((2, channels, BLK), BF16),
                vmem((2, channels, BLK), BF16),
                vmem((2 * channels, 3 * BLK), BF16),
                vmem((2, half_features, 2 * BLK), BF16),
                pltpu.SemaphoreType.DMA((21,)),
                pltpu.SemaphoreType.DMA((17,)),
                pltpu.SemaphoreType.DMA((17,)),
                pltpu.SemaphoreType.REGULAR,
            ],
            compiler_params=pltpu.CompilerParams(
                collective_id=0, has_side_effects=True, vmem_limit_bytes=60 * 1024 * 1024
            ),
        )(
            stream, norm_gain, w_value, w_gate, jnp.transpose(conv_taps, (2, 0, 1)),
            group_gain, group_shift, w_out, *tables(taps),
        )
        return write_out(result)

    placed = (
        P("tp", "sp"),
        P(),
        P(None, "tp", None),
        P(None, "tp", None),
        P(None, "tp", None),
        P(None, "tp"),
        P(None, "tp"),
        P(None, "tp", None),
    )
    return jax.shard_map(body, mesh=mesh, in_specs=placed, out_specs=P("tp", "sp"), check_vma=False)
```

time: 27.8 us -> 22.4 us (0.81)
  local copies, waits for them, and re-layouts: 3.69 us -> 0 us
  Pallas kernels: 24 us -> 22.3 us
    unnamed x2 -> x0, local copies, waits for them, and re-layouts: 3.69 us -> none
    pallas_call x1 -> x2, Pallas kernels: 24 us -> 22.3 us  [the longest x1 21.5 us: body(): pl.pallas_call(functools.partial(kernel, n_sp), out_shape=pltpu.VMEM(stre...]
where the time goes in v3:
time: 22.4 us; the launch traced here: 22.3 us
  Pallas kernels  22.3 us (100%)
    pallas_call x1, Pallas kernels, body(): pl.pallas_call(functools.partial(kernel, n_sp), out_shape=pltpu.VMEM(stre...  21.5 us
    pallas_call x1, Pallas kernels, write_out(): pl.pallas_call(write_kernel, out_shape=jax.ShapeDtypeStruct(value.shape,...  0.8 us

profile of v3, /device:TPU:385, one launch (start us, length us, event | category | flops | bytes accessed | tf_op | source)
XLA Modules:
  0.0 22.3 jit_solution(12462770107312103425)
XLA Ops:
  0.0 21.5 %shard_map.109.src = bf16[512,512]{1,0:T(8,128)(2,1)S(1)} custom-call(bf16[512,512]{1,0:T(8,128)(2,1)} %x_hbm.1, f32[2,1024]{1,0:T(2,128)} %ng_hbm.1, bf16[2,256,1024]{2,1,0:T(8,128)(2,1)} %wv_hbm.1, bf16[2,256,1024]{2,1,0:T(8,128)(2,1)} %wg_hbm.1, bf16[255,2,256]{2,1,0:T(2,128)(2,1)} %bitcast.1, f32[2,256]{1,0:T(2,128)} %gg_hbm.1, f32[2,256]{1,0:T(2,128)} %gs_hbm.1, ...), custom_call_target="tpu_custom_call" | custom-call | tf_op jit(solution)/shard_map/pallas_call | solution.py:365
  21.5 0.8 %shard_map.110 = bf16[512,512]{1,0:T(8,128)(2,1)} custom-call(bf16[512,512]{1,0:T(8,128)(2,1)S(1)} %shard_map.109.src), custom_call_target="tpu_custom_call" | custom-call | tf_op jit(solution)/shard_map/pallas_call | solution.py:345

commit v4 on v3

--- a/solution.py
+++ b/solution.py
@@ -85,6 +85,52 @@
         load("x", x_hbm.at[:, pl.ds(b * BLK, BLK)], xin.at[b])
     load("ng", ng_hbm, ngv)
     load_wvg(0)
+
+    NEAR, FAR, XMID, XINN, WVG, WO, RESP, GG, GS, PAR1, PAR2, OMID = 0, 2, 3, 4, 5, 7, 9, 11, 12, 13, 14, 15
+    sent = []
+
+    def remote(k, src, dst, device):
+        return pltpu.make_async_remote_copy(
+            src_ref=src, dst_ref=dst, send_sem=ssem.at[k], recv_sem=rsem.at[k],
+            device_id=device, device_id_type=MESH,
+        )
+
+    def to_partner(k, src, dst):
+        copy = remote(k, src, dst, (sp, p))
+        copy.start()
+        sent.append(copy)
+
+    def from_partner(k, dst):
+        remote(k, dst, dst, (sp, p)).wait_recv()
+
+    def scale_weights(l):
+        gain = ngv[l : l + 1]
+        for k in range(2):
+            for half in range(2):
+                wvg[l, c, k, half] = (wraw[l, k, half].astype(F32) * gain).astype(BF16)
+
+    def spread_groups(h):
+        column = lambda row: jnp.broadcast_to(row * 0.5, (BLK, BLK)).T
+        for l in range(layers):
+            for b in range(2):
+                lanes = slice(b * BLK, (b + 1) * BLK)
+                ggb[l, h, lanes] = column(ggv[h, l : l + 1, lanes])
+                gsb[l, h, lanes] = column(gsv[h, l : l + 1, lanes])
+
+    loaded("x")
+
+    @pl.when(c == 0)
+    def _():
+        pl.semaphore_wait(barrier, 1)
+        pl.semaphore_signal(ready, inc=1, device_id=(sp, 1), device_id_type=MESH)
+
+    @pl.when(c == 1)
+    def _():
+        pl.semaphore_wait(ready, 1)
+
+    mid, inn = pl.ds(BLK, BLK), pl.ds(2 * BLK, BLK)
+    to_partner(XINN, xin.at[1 + p], xs.at[c, :, inn])
+    to_partner(XMID, xin.at[3 * p], xs.at[c, :, mid])
     load("groups", gg_hbm, ggv.at[c])
     load("groups", gs_hbm, gsv.at[c])
     load("taps", taps_hbm, taps.at[pl.ds(0, taps_hbm.shape[0])])
@@ -94,52 +140,6 @@
     load("wo0", wo_hbm.at[0], wo.at[0, c])
     load_wvg(1)
     load("wo1", wo_hbm.at[1], wo.at[1, c])
-
-    NEAR, FAR, XMID, XINN, WVG, WO, RESP, GG, GS, PAR1, PAR2, OMID = 0, 2, 3, 4, 5, 7, 9, 11, 12, 13, 14, 15
-    sent = []
-
-    def remote(k, src, dst, device):
-        return pltpu.make_async_remote_copy(
-            src_ref=src, dst_ref=dst, send_sem=ssem.at[k], recv_sem=rsem.at[k],
-            device_id=device, device_id_type=MESH,
-        )
-
-    def to_partner(k, src, dst):
-        copy = remote(k, src, dst, (sp, p))
-        copy.start()
-        sent.append(copy)
-
-    def from_partner(k, dst):
-        remote(k, dst, dst, (sp, p)).wait_recv()
-
-    def scale_weights(l):
-        gain = ngv[l : l + 1]
-        for k in range(2):
-            for half in range(2):
-                wvg[l, c, k, half] = (wraw[l, k, half].astype(F32) * gain).astype(BF16)
-
-    def spread_groups(h):
-        column = lambda row: jnp.broadcast_to(row * 0.5, (BLK, BLK)).T
-        for l in range(layers):
-            for b in range(2):
-                lanes = slice(b * BLK, (b + 1) * BLK)
-                ggb[l, h, lanes] = column(ggv[h, l : l + 1, lanes])
-                gsb[l, h, lanes] = column(gsv[h, l : l + 1, lanes])
-
-    loaded("x")
-
-    @pl.when(c == 0)
-    def _():
-        pl.semaphore_wait(barrier, 1)
-        pl.semaphore_signal(ready, inc=1, device_id=(sp, 1), device_id_type=MESH)
-
-    @pl.when(c == 1)
-    def _():
-        pl.semaphore_wait(ready, 1)
-
-    mid, inn = pl.ds(BLK, BLK), pl.ds(2 * BLK, BLK)
-    to_partner(XINN, xin.at[1 + p], xs.at[c, :, inn])
-    to_partner(XMID, xin.at[3 * p], xs.at[c, :, mid])
     loaded("ng", "w0")
     scale_weights(0)
     loaded("groups")
@@ -238,6 +238,7 @@
             project_out(l, h, lanes, xs.at[h], lanes)
 
     own, outside = slice(BLK, 3 * BLK), slice(0, BLK)
+    inner, outward = slice(2 * BLK, 3 * BLK), slice(0, 2 * BLK)
 
     from_partner(XINN, xs.at[p, :, inn])
     from_partner(XMID, xs.at[p, :, mid])
@@ -266,6 +267,15 @@
     to_partner(WO + 1, wo.at[1, c], wo.at[1, c])
     loaded("tables")
 
+    from_partner(RESP, resp.at[0, p])
+    from_partner(PAR1, gpar1)
+    filter_norm(0, lambda h: jnp.concatenate([g1[h, :, own], gpar1[h]], axis=1), slice(0, BLK), inner)
+    from_partner(WO, wo.at[0, p])
+    advance(0, inner)
+    from_partner(WVG + 1, wvg.at[1, p])
+    gate(1, (0, 1), inner, g2, half_inverse(inner))
+    to_partner(PAR2, g2.at[:, :, inn], gpar2)
+
     @pl.when(has_outer)
     def _():
         for core in range(2):
@@ -282,28 +292,20 @@
 
     gate(0, (0, 1), outside, g1, half_inverse(outside))
 
-    from_partner(RESP, resp.at[0, p])
-    from_partner(PAR1, gpar1)
-    filter_norm(0, lambda h: jnp.concatenate([g1[h], gpar1[h]], axis=1), slice(0, 2 * BLK), own)
-    from_partner(WO, wo.at[0, p])
-    advance(0, own)
-
-    from_partner(WVG + 1, wvg.at[1, p])
-    gate(1, (0, 1), own, g2, half_inverse(own))
-    to_partner(PAR2, g2.at[:, :, inn], gpar2)
+    from_partner(RESP + 1, resp.at[1, p])
+    from_partner(WO + 1, wo.at[1, p])
+    from_partner(PAR2, gpar2)
 
     @pl.when(has_outer)
     def _():
         remote(FAR, gfar, gfar, (outer, p)).wait_recv()
 
-    filter_norm(0, lambda h: jnp.concatenate([gfar[h], g1[h, :, : 2 * BLK]], axis=1), slice(0, BLK), outside)
-    advance(0, outside)
-
-    gate(1, (0, 1), outside, g2, half_inverse(outside), jnp.where(has_outer, 1.0, 0.0))
-    from_partner(RESP + 1, resp.at[1, p])
-    from_partner(PAR2, gpar2)
+    filter_norm(0, lambda h: jnp.concatenate([gfar[h], g1[h]], axis=1), slice(0, 2 * BLK), outward)
+    advance(0, outward)
+    exists = jnp.where(has_outer, 1.0, 0.0)
+    exists = jnp.concatenate([jnp.full((1, BLK), exists, F32), jnp.ones((1, BLK), F32)], axis=1)
+    gate(1, (0, 1), outward, g2, half_inverse(outward), exists)
     filter_norm(1, lambda h: jnp.concatenate([g2[h], gpar2[h]], axis=1), slice(0, 2 * BLK), own)
-    from_partner(WO + 1, wo.at[1, p])
 
     columns = lambda core: (
         pl.ds(pl.multiple_of(core * 3 * BLK, BLK), BLK),

time: 22.4 us -> 23.1 us (1.031)
  the two profiles are of different devices: /device:TPU:385 before, /device:TPU:1 now
where the time goes in v4:
time: 23.1 us; the launch traced here: 23 us
  Pallas kernels  22.9 us (99%)
    pallas_call x1, Pallas kernels, body(): pl.pallas_call(functools.partial(kernel, n_sp), out_shape=pltpu.VMEM(stre...  22.1 us
    pallas_call x1, Pallas kernels, write_out(): pl.pallas_call(write_kernel, out_shape=jax.ShapeDtypeStruct(value.shape,...  0.8 us

profile of v4, /device:TPU:1, one launch (start us, length us, event | category | flops | bytes accessed | tf_op | source)
XLA Modules:
  0.0 23.0 jit_solution(6945747818245657681)
XLA Ops:
  0.0 22.1 %shard_map.109.src = bf16[512,512]{1,0:T(8,128)(2,1)S(1)} custom-call(bf16[512,512]{1,0:T(8,128)(2,1)} %x_hbm.1, f32[2,1024]{1,0:T(2,128)} %ng_hbm.1, bf16[2,256,1024]{2,1,0:T(8,128)(2,1)} %wv_hbm.1, bf16[2,256,1024]{2,1,0:T(8,128)(2,1)} %wg_hbm.1, bf16[255,2,256]{2,1,0:T(2,128)(2,1)} %bitcast.1, f32[2,256]{1,0:T(2,128)} %gg_hbm.1, f32[2,256]{1,0:T(2,128)} %gs_hbm.1, ...), custom_call_target="tpu_custom_call" | custom-call | tf_op jit(solution)/shard_map/pallas_call | solution.py:367
  22.1 0.8 %shard_map.110 = bf16[512,512]{1,0:T(8,128)(2,1)} custom-call(bf16[512,512]{1,0:T(8,128)(2,1)S(1)} %shard_map.109.src), custom_call_target="tpu_custom_call" | custom-call | tf_op jit(solution)/shard_map/pallas_call | solution.py:347

commit v5 on v4

v5 whole, which is shorter than its diff:
```python
import functools

import jax
import jax.numpy as jnp
import numpy as np
from jax import lax
from jax.experimental import pallas as pl
from jax.experimental.pallas import tpu as pltpu
from jax.sharding import PartitionSpec as P

MESH = pl.DeviceIdType.MESH
BLK = 128
SIZE = 512
HALF = SIZE // 2
RMS_EPS = 1e-06
LN_EPS = 1e-05
F32 = jnp.float32
BF16 = jnp.bfloat16


def tables(taps):
    angle = lambda t: np.asarray(t)[:, None] * ((np.arange(HALF) + 0.5) * (2 * np.pi / SIZE))[None]
    trig = lambda t: np.concatenate([np.cos(angle(t)), np.sin(angle(t))], axis=1)
    blocks = [np.arange(BLK) + BLK * b for b in range(4)]
    reach = (taps - 1) // 2
    forward = [np.concatenate([trig(blocks[b]) for b in order]) for order in ((0, 1, 2, 3), (3, 2, 1, 0))]
    back = [
        np.concatenate([trig(blocks[b] - reach).T for b in order], axis=1) * (2.0 / SIZE)
        for order in ((1, 2), (2, 1))
    ]
    mixed = np.zeros((2, 2 * BLK, 2, 2 * HALF))
    for layer in range(2):
        mixed[layer, :taps, layer] = trig(np.arange(taps))
    return (
        jnp.asarray(np.stack(forward), BF16),
        jnp.asarray(np.stack(back), BF16),
        jnp.asarray(mixed.reshape(2, 4 * BLK, SIZE), BF16),
    )


def kernel(
    n_sp,
    x_hbm, ng_hbm, wv_hbm, wg_hbm, taps_hbm, gg_hbm, gs_hbm, wo_hbm, fwd_hbm, back_hbm, ftap_hbm,
    o_ref,
    xall, xs, wraw, wvg, wo, taps, ngv, gv, ggb, gsb, resp, fwd, back, ftap,
    acc, gall, g1, g2, gfar, gpar1, gpar2, act, obuf,
    rsem, ready, lsem, ssem,
):
    sp, c = lax.axis_index("sp"), lax.axis_index("tp")
    p = 1 - c
    outer = sp + 2 * c - 1
    has_left = sp > 0
    has_right = sp < n_sp - 1
    has_outer = jnp.logical_and(outer >= 0, outer < n_sp)
    early = jnp.logical_and(sp == 0, c == 1)
    later = jnp.logical_not(early)
    left_count = jnp.where(has_left, 1, 0)
    right_count = jnp.where(has_right, 1, 0)
    layers, features = ng_hbm.shape

    local = {}

    def load(name, pairs, whole):
        sem = lsem.at[len(local)]
        for src, dst in pairs:
            pltpu.make_async_copy(src, dst, sem).start()
        local[name] = pltpu.make_async_copy(whole, whole, sem)

    def loaded(*names):
        for name in names:
            local[name].wait()

    def load_wvg(l):
        pairs = []
        for k in range(2):
            pairs.append((wv_hbm.at[l, pl.ds(k * BLK, BLK)], wraw.at[l, k, 0]))
            pairs.append((wg_hbm.at[l, pl.ds(k * BLK, BLK)], wraw.at[l, k, 1]))
        load(f"w{l}", pairs, wraw.at[l])

    load("x", [(x_hbm.at[:, pl.ds(b * BLK, BLK)], xall.at[c, b]) for b in range(4)], xall.at[c])

    barrier = pltpu.get_barrier_semaphore()
    pl.semaphore_signal(barrier, inc=1, device_id=(sp, p), device_id_type=MESH)

    @pl.when(has_outer)
    def _():
        pl.semaphore_signal(barrier, inc=1, device_id=(outer, 1), device_id_type=MESH)

    load("ng", [(ng_hbm, ngv)], ngv)
    load_wvg(0)
    load("groups", [(gg_hbm, gv.at[c, 0]), (gs_hbm, gv.at[c, 1])], gv.at[c])
    load("wo0", [(wo_hbm.at[0], wo.at[0, c])], wo.at[0, c])
    tap_rows = taps.at[pl.ds(0, taps_hbm.shape[0])]
    load("taps", [(taps_hbm, tap_rows)], tap_rows)
    load("ftap", [(ftap_hbm, ftap)], ftap)
    load_wvg(1)
    load("fwd", [(fwd_hbm.at[c], fwd)], fwd)
    load("back", [(back_hbm.at[c], back)], back)
    load("wo1", [(wo_hbm.at[1], wo.at[1, c])], wo.at[1, c])

    NEAR, FAR, X, GMID, GINN, WVG, WO, RESP, GV, PAR1, PAR2, OMID = 0, 2, 4, 5, 6, 7, 10, 12, 14, 15, 16, 17
    sent = []

    def remote(k, src, dst, device):
        return pltpu.make_async_remote_copy(
            src_ref=src, dst_ref=dst, send_sem=ssem.at[k], recv_sem=rsem.at[k],
            device_id=device, device_id_type=MESH,
        )

    def to_partner(k, src, dst, when=None):
        copy = remote(k, src, dst, (sp, p))
        if when is None:
            copy.start()
        else:
            pl.when(when)(copy.start)
        if when is not later:
            sent.append(copy)

    def share(ref, k, l, when=None):
        to_partner(k + l, ref.at[l, c], ref.at[l, c], when)

    def from_partner(k, dst):
        remote(k, dst, dst, (sp, p)).wait_recv()

    def to_neighbour(first, direction, src, dst):
        return pltpu.make_async_remote_copy(
            src_ref=src, dst_ref=dst, send_sem=ssem.at[first + direction], recv_sem=rsem.at[first + c],
            device_id=(sp + 2 * direction - 1, 1 - direction), device_id_type=MESH,
        )

    def from_outer(first, part):
        for core in range(2):
            dst = part(core)
            pltpu.make_async_remote_copy(
                src_ref=dst, dst_ref=dst, send_sem=ssem.at[first], recv_sem=rsem.at[first + core],
                device_id=(outer, core), device_id_type=MESH,
            ).wait_recv()

    def start_both(copies):
        for there, copy in zip((has_left, has_right), copies):
            pl.when(there)(copy.start)

    def scale_weights(l):
        gain = ngv[l : l + 1]
        for k in range(2):
            for half in range(2):
                wvg[l, c, k, half] = (wraw[l, k, half].astype(F32) * gain).astype(BF16)

    def spread_groups(h):
        column = lambda row: jnp.broadcast_to(row * 0.5, (BLK, BLK)).T
        for l in range(layers):
            for b in range(2):
                lanes = slice(b * BLK, (b + 1) * BLK)
                ggb[l, h, lanes] = column(gv[h, 0, l : l + 1, lanes])
                gsb[l, h, lanes] = column(gv[h, 1, l : l + 1, lanes])

    def prepare_gates():
        loaded("groups", "ng", "w0")
        scale_weights(0)

    def prepare_taps():
        loaded("taps", "ftap")
        taps[taps_hbm.shape[0] :] = jnp.zeros((taps.shape[0] - taps_hbm.shape[0], *taps.shape[1:]), BF16)

    def respond(l):
        rows = taps[...].reshape(layers * taps.shape[0], taps.shape[2])
        resp[l, c] = lax.dot_general(
            rows, ftap[l], (((0,), (0,)), ((), ())), preferred_element_type=F32
        ).astype(BF16)

    def prepare_weights():
        loaded("w1")
        scale_weights(1)

    @pl.when(early)
    def _():
        prepare_gates()
        prepare_taps()
        for l in range(layers):
            respond(l)
        prepare_weights()
        spread_groups(c)

    @pl.when(c == 0)
    def _():
        pl.semaphore_wait(barrier, 1)
        pl.semaphore_signal(ready, inc=1, device_id=(sp, 1), device_id_type=MESH)

    @pl.when(c == 1)
    def _():
        pl.semaphore_wait(ready, 1)

    loaded("x")
    to_partner(X, xall.at[c], xall.at[c])

    @pl.when(c == 1)
    def _():
        pl.semaphore_wait(barrier, 1 + left_count + right_count)
        pl.semaphore_signal(ready, inc=1, device_id=(sp, 0), device_id_type=MESH)

    @pl.when(c == 0)
    def _():
        pl.semaphore_wait(ready, 1)

    near = (slice(None), pl.ds(0, BLK))
    near_copies = [to_neighbour(NEAR, d, xall.at[c, 3 * d], xs.at[(c, *near)]) for d in range(2)]
    start_both(near_copies)

    pl.when(later)(prepare_gates)
    to_partner(GV, gv.at[c], gv.at[c])
    loaded("wo0")
    share(wo, WO, 0)
    for l in range(layers):
        share(resp, RESP, l, early)

    def squares(x):
        wide = x.astype(F32)
        return jnp.sum(wide * wide, axis=0, keepdims=True)

    def half_inverse(total):
        return 0.5 * lax.rsqrt(total * (1.0 / features) + RMS_EPS)

    def gated(r, inverse, kept):
        value = r[:BLK] * kept
        return (value * jnp.tanh(r[BLK:] * inverse) + value).astype(BF16)

    def gate(l, lanes, dst, exists=None, arrived=None):
        x = xs[:, :, lanes].reshape(features, lanes.stop - lanes.start)
        inverse = half_inverse(squares(x))
        kept = inverse if exists is None else inverse * exists
        for h in range(2) if arrived is None else (c, p):
            if h is p:
                arrived()
            for k in range(2):
                r = jnp.dot(wvg[l, h, k].reshape(2 * BLK, features), x, preferred_element_type=F32)
                dst[h, k * BLK : (k + 1) * BLK, lanes] = gated(r, inverse, kept)

    def filter_norm(l, window, outputs, lanes, halves=(0, 1)):
        n = outputs.stop - outputs.start
        for h in halves:
            w = window(h)
            g = jnp.dot(w, fwd[: w.shape[1]], preferred_element_type=F32)
            gr, gi = g[:, :HALF], g[:, HALF:]
            hr, hi = resp[l, h, :, :HALF].astype(F32), resp[l, h, :, HALF:].astype(F32)
            y = jnp.concatenate([(gr * hr + gi * hi).astype(BF16), (gi * hr - gr * hi).astype(BF16)], axis=1)
            filtered = jnp.dot(y, back[:, outputs], preferred_element_type=F32)
            for k in range(2):
                part = slice(k * BLK, (k + 1) * BLK)
                f = filtered[part]
                centred = f - jnp.sum(f, axis=0, keepdims=True) * (1.0 / BLK)
                variance = jnp.sum(centred * centred, axis=0, keepdims=True) * (1.0 / BLK)
                gain, shift = ggb[l, h, part], gsb[l, h, part]
                if n > BLK:
                    gain = jnp.concatenate([gain] * (n // BLK), axis=1)
                    shift = jnp.concatenate([shift] * (n // BLK), axis=1)
                s = centred * lax.rsqrt(variance + LN_EPS) * gain + shift
                act[h, part, lanes] = (s * jnp.tanh(s) + s).astype(BF16)

    def project_out(l, h, lanes, dst, dst_lanes, pieces=((0, 2 * BLK), (2 * BLK, 2 * BLK))):
        for first, size in pieces:
            part = slice(first, first + size)
            activated = act[:, :, lanes].reshape(wo.shape[3], lanes.stop - lanes.start)
            branch = jnp.dot(wo[l, h, part], activated, preferred_element_type=F32)
            dst[part, dst_lanes] = (xs[h, part, lanes].astype(F32) + branch).astype(BF16)

    def advance(l, lanes):
        for h in range(2):
            project_out(l, h, lanes, xs.at[h], lanes)

    own, outside = slice(BLK, 3 * BLK), slice(0, BLK)
    inner, outward = slice(2 * BLK, 3 * BLK), slice(0, 2 * BLK)

    part_rows = features // 2

    def part_dot(core, k):
        x = jnp.concatenate([xall[core, b] for b in range(4)], axis=1)
        w = wvg[0, c, k, :, :, pl.ds(pl.multiple_of(core * part_rows, part_rows), part_rows)]
        return jnp.dot(w.reshape(2 * BLK, part_rows), x, preferred_element_type=F32)

    def part_squares(core):
        return jnp.concatenate([squares(xall[core, b]) for b in range(4)], axis=1)

    for k in range(2):
        acc[k] = part_dot(c, k)
    total = part_squares(c)
    from_partner(X, xall.at[p])
    inverse = half_inverse(total + part_squares(p))
    for k in range(2):
        gk = gated(acc[k] + part_dot(p, k), inverse, inverse)
        for b in range(4):
            gall[b, k * BLK : (k + 1) * BLK] = gk[:, b * BLK : (b + 1) * BLK]
    mid, inn = pl.ds(BLK, BLK), pl.ds(2 * BLK, BLK)
    to_partner(GINN, gall.at[1 + p], g1.at[c, :, inn])
    to_partner(PAR1, gall.at[1 + c], gpar1.at[c])
    to_partner(GMID, gall.at[3 * p], g1.at[c, :, mid])
    far_copies = [to_neighbour(FAR, d, gall.at[1 + d], gfar.at[c]) for d in range(2)]
    start_both(far_copies)

    @pl.when(later)
    def _():
        prepare_taps()
        respond(0)

    share(resp, RESP, 0, later)
    pl.when(later)(prepare_weights)
    share(wvg, WVG, 1)
    share(wvg, WVG, 0)
    for h in range(2):
        xs[h, :, BLK : 2 * BLK] = xall[h, 3 * c]
        xs[h, :, 2 * BLK : 3 * BLK] = xall[h, 1 + c]
    g1[c, :, BLK : 2 * BLK] = gall[3 * c]
    g1[c, :, 2 * BLK : 3 * BLK] = gall[1 + c]
    gpar1[c] = gall[1 + p]

    loaded("fwd", "back")

    @pl.when(later)
    def _():
        spread_groups(c)

    inner_window = lambda h: jnp.concatenate([g1[h, :, own], gpar1[h]], axis=1)
    filter_norm(0, inner_window, slice(0, BLK), inner, (c,))
    from_partner(GV, gv.at[p])
    spread_groups(p)

    from_partner(RESP, resp.at[0, p])
    from_partner(WO, wo.at[0, p])
    from_partner(GINN, g1.at[p, :, inn])
    from_partner(PAR1, gpar1.at[p])
    from_partner(GMID, g1.at[p, :, mid])
    filter_norm(0, inner_window, slice(0, BLK), inner, (p,))
    advance(0, inner)
    from_partner(WVG + 1, wvg.at[1, p])
    gate(1, inner, g2)
    to_partner(PAR2, g2.at[:, :, inn], gpar2)
    pl.when(later)(lambda: respond(1))
    share(resp, RESP, 1, later)
    loaded("wo1")
    share(wo, WO, 1)

    @pl.when(has_outer)
    def _():
        from_outer(NEAR, lambda core: xs.at[(core, *near)])
        gate(0, outside, g1, arrived=lambda: from_partner(WVG, wvg.at[0, p]))

    @pl.when(jnp.logical_not(has_outer))
    def _():
        from_partner(WVG, wvg.at[0, p])
        xs[:, :, outside] = jnp.zeros((2, xs.shape[1], BLK), BF16)
        g1[:, :, outside] = jnp.zeros_like(gfar)
        gfar[...] = jnp.zeros_like(gfar)

    @pl.when(has_outer)
    def _():
        from_outer(FAR, lambda core: gfar.at[core])

    filter_norm(0, lambda h: jnp.concatenate([gfar[h], g1[h]], axis=1), slice(0, 2 * BLK), outward)
    advance(0, outward)
    exists = jnp.where(has_outer, 1.0, 0.0)
    gate(1, outward, g2, jnp.concatenate([jnp.full((1, BLK), exists, F32), jnp.ones((1, BLK), F32)], axis=1))
    from_partner(PAR2, gpar2)
    from_partner(RESP + 1, resp.at[1, p])
    from_partner(WO + 1, wo.at[1, p])
    filter_norm(1, lambda h: jnp.concatenate([g2[h], gpar2[h]], axis=1), slice(0, 2 * BLK), own)

    columns = lambda core: (
        pl.ds(pl.multiple_of(core * 3 * BLK, BLK), BLK),
        pl.ds(pl.multiple_of((1 + core) * BLK, BLK), BLK),
    )
    whole = slice(0, 2 * BLK)
    pairs = [tuple((2 * q * BLK + r * BLK, BLK) for r in range(2)) for q in range(2)]
    for q in range(2):
        project_out(1, p, own, obuf.at[0], whole, pairs[q])
        part = pl.ds(2 * q * BLK, 2 * BLK)
        for k, lane in enumerate(columns(c)):
            to_partner(OMID + 2 * q + k, obuf.at[0, part, pl.ds(k * BLK, BLK)], o_ref.at[part, lane])
    project_out(1, c, own, obuf.at[1], whole)
    for k, lane in enumerate(columns(c)):
        o_ref[:, lane] = obuf[1, :, k * BLK : (k + 1) * BLK]
    for copies in (near_copies, far_copies):
        for there, copy in zip((has_left, has_right), copies):
            pl.when(there)(copy.wait_send)
    for copy in sent:
        copy.wait_send()
    for q in range(2):
        part = pl.ds(2 * q * BLK, 2 * BLK)
        for k, lane in enumerate(columns(p)):
            from_partner(OMID + 2 * q + k, o_ref.at[part, lane])


def scoped(n_sp, *refs):
    pl.run_scoped(
        lambda *semaphores: kernel(n_sp, *refs, *semaphores),
        pltpu.SemaphoreType.DMA((11,)),
        pltpu.SemaphoreType.DMA((21,)),
    )


def write_kernel(src, dst, sem):
    copy = pltpu.make_async_copy(src, dst, sem)
    copy.start()
    copy.wait()


def write_out(value):
    return pl.pallas_call(
        write_kernel,
        out_shape=jax.ShapeDtypeStruct(value.shape, value.dtype),
        in_specs=[pl.BlockSpec(memory_space=pltpu.VMEM)],
        out_specs=pl.BlockSpec(memory_space=pl.ANY),
        scratch_shapes=[pltpu.SemaphoreType.DMA],
        compiler_params=pltpu.CompilerParams(vmem_limit_bytes=1024 * 1024),
    )(pltpu.with_memory_space_constraint(value, pltpu.VMEM))


def solution(mesh):
    n_sp = mesh.shape["sp"]

    def body(stream, norm_gain, w_value, w_gate, conv_taps, group_gain, group_shift, w_out):
        layers, features = norm_gain.shape
        half_features, tokens = stream.shape
        channels = w_value.shape[1]
        taps = conv_taps.shape[2]
        any_spec = pl.BlockSpec(memory_space=pl.ANY)
        vmem = pltpu.VMEM
        result = pl.pallas_call(
            functools.partial(scoped, n_sp),
            out_shape=pltpu.VMEM(stream.shape, stream.dtype),
            in_specs=[any_spec] * 11,
            out_specs=pl.BlockSpec(memory_space=pltpu.VMEM),
            scratch_shapes=[
                vmem((2, 4, half_features, BLK), BF16),
                vmem((2, half_features, 3 * BLK), BF16),
                vmem((layers, 2, 2, BLK, features), BF16),
                vmem((layers, 2, 2, 2, BLK, features), BF16),
                vmem((layers, 2, half_features, 2 * channels), BF16),
                vmem((2 * BLK, layers, channels), BF16),
                vmem((layers, features), F32),
                vmem((2, 2, layers, channels), F32),
                vmem((layers, 2, channels, BLK), F32),
                vmem((layers, 2, channels, BLK), F32),
                vmem((layers, 2, channels, SIZE), BF16),
                vmem((SIZE, SIZE), BF16),
                vmem((SIZE, 2 * BLK), BF16),
                vmem((layers, SIZE, SIZE), BF16),
                vmem((2, 2 * BLK, tokens), F32),
                vmem((4, channels, BLK), BF16),
                vmem((2, channels, 3 * BLK), BF16),
                vmem((2, channels, 3 * BLK), BF16),
                vmem((2, channels, BLK), BF16),
                vmem((2, channels, BLK), BF16),
                vmem((2, channels, BLK), BF16),
                vmem((2, channels, 3 * BLK), BF16),
                vmem((2, half_features, 2 * BLK), BF16),
                pltpu.SemaphoreType.DMA((21,)),
                pltpu.SemaphoreType.REGULAR,
            ],
            compiler_params=pltpu.CompilerParams(
                collective_id=0, has_side_effects=True, vmem_limit_bytes=60 * 1024 * 1024
            ),
        )(
            stream, norm_gain, w_value, w_gate, jnp.transpose(conv_taps, (2, 0, 1)),
            group_gain, group_shift, w_out, *tables(taps),
        )
        return write_out(result)

    placed = (
        P("tp", "sp"),
        P(),
        P(None, "tp", None),
        P(None, "tp", None),
        P(None, "tp", None),
        P(None, "tp"),
        P(None, "tp"),
        P(None, "tp", None),
    )
    return jax.shard_map(body, mesh=mesh, in_specs=placed, out_specs=P("tp", "sp"), check_vma=False)
```

time: 23.1 us -> 20.4 us (0.88)
  Pallas kernels: 22.9 us -> 20.3 us
    pallas_call x1, Pallas kernels: 22.1 us -> 19.5 us  [body(): pl.pallas_call(functools.partial(scoped, n_sp), out_shape=pltpu.VMEM(stre...]
where the time goes in v5:
time: 20.4 us; the launch traced here: 20.3 us
  Pallas kernels  20.3 us (100%)
    pallas_call x1, Pallas kernels, body(): pl.pallas_call(functools.partial(scoped, n_sp), out_shape=pltpu.VMEM(stre...  19.5 us
    pallas_call x1, Pallas kernels, write_out(): pl.pallas_call(write_kernel, out_shape=jax.ShapeDtypeStruct(value.shape,...  0.8 us

profile of v5, /device:TPU:1, one launch (start us, length us, event | category | flops | bytes accessed | tf_op | source)
XLA Modules:
  0.0 20.3 jit_solution(16610070186661275623)
XLA Ops:
  0.0 19.5 %shard_map.109.src = bf16[512,512]{1,0:T(8,128)(2,1)S(1)} custom-call(bf16[512,512]{1,0:T(8,128)(2,1)} %refs_0_.1, f32[2,1024]{1,0:T(2,128)} %refs_1_.1, bf16[2,256,1024]{2,1,0:T(8,128)(2,1)} %refs_2_.1, bf16[2,256,1024]{2,1,0:T(8,128)(2,1)} %refs_3_.1, bf16[255,2,256]{2,1,0:T(2,128)(2,1)} %bitcast.1, f32[2,256]{1,0:T(2,128)} %refs_5_.1, f32[2,256]{1,0:T(2,128)} %refs_6_.1, ...), custom_call_target="tpu_custom_call" | custom-call | tf_op jit(solution)/shard_map/pallas_call | solution.py:426
  19.5 0.8 %shard_map.110 = bf16[512,512]{1,0:T(8,128)(2,1)} custom-call(bf16[512,512]{1,0:T(8,128)(2,1)S(1)} %shard_map.109.src), custom_call_target="tpu_custom_call" | custom-call | tf_op jit(solution)/shard_map/pallas_call | solution.py:406

commit v6 on v5

--- a/solution.py
+++ b/solution.py
@@ -20,7 +20,9 @@
 
 def tables(taps):
     angle = lambda t: np.asarray(t)[:, None] * ((np.arange(HALF) + 0.5) * (2 * np.pi / SIZE))[None]
-    trig = lambda t: np.concatenate([np.cos(angle(t)), np.sin(angle(t))], axis=1)
+    trig = lambda t: np.stack([np.cos(angle(t)), np.sin(angle(t))], axis=1).reshape(
+        -1, 2, 2, BLK
+    ).transpose(0, 2, 1, 3).reshape(-1, SIZE)
     blocks = [np.arange(BLK) + BLK * b for b in range(4)]
     reach = (taps - 1) // 2
     forward = [np.concatenate([trig(blocks[b]) for b in order]) for order in ((0, 1, 2, 3), (3, 2, 1, 0))]
@@ -43,7 +45,7 @@
     x_hbm, ng_hbm, wv_hbm, wg_hbm, taps_hbm, gg_hbm, gs_hbm, wo_hbm, fwd_hbm, back_hbm, ftap_hbm,
     o_ref,
     xall, xs, wraw, wvg, wo, taps, ngv, gv, ggb, gsb, resp, fwd, back, ftap,
-    acc, gall, g1, g2, gfar, gpar1, gpar2, act, obuf,
+    acc, gall, g1, g2, gfar, gnear, gpar1, gpar2, act, obuf,
     rsem, ready, lsem, ssem,
 ):
     sp, c = lax.axis_index("sp"), lax.axis_index("tp")
@@ -52,8 +54,11 @@
     has_left = sp > 0
     has_right = sp < n_sp - 1
     has_outer = jnp.logical_and(outer >= 0, outer < n_sp)
-    early = jnp.logical_and(sp == 0, c == 1)
+    first = sp == 0
+    head = jnp.logical_and(first, c == 0)
+    early = jnp.logical_and(first, c == 1)
     later = jnp.logical_not(early)
+    past = sp > 0
     left_count = jnp.where(has_left, 1, 0)
     right_count = jnp.where(has_right, 1, 0)
     layers, features = ng_hbm.shape
@@ -87,8 +92,8 @@
         pl.semaphore_signal(barrier, inc=1, device_id=(outer, 1), device_id_type=MESH)
 
     load("ng", [(ng_hbm, ngv)], ngv)
+    load("groups", [(gg_hbm, gv.at[c, 0]), (gs_hbm, gv.at[c, 1])], gv.at[c])
     load_wvg(0)
-    load("groups", [(gg_hbm, gv.at[c, 0]), (gs_hbm, gv.at[c, 1])], gv.at[c])
     load("wo0", [(wo_hbm.at[0], wo.at[0, c])], wo.at[0, c])
     tap_rows = taps.at[pl.ds(0, taps_hbm.shape[0])]
     load("taps", [(taps_hbm, tap_rows)], tap_rows)
@@ -98,7 +103,8 @@
     load("back", [(back_hbm.at[c], back)], back)
     load("wo1", [(wo_hbm.at[1], wo.at[1, c])], wo.at[1, c])
 
-    NEAR, FAR, X, GMID, GINN, WVG, WO, RESP, GV, PAR1, PAR2, OMID = 0, 2, 4, 5, 6, 7, 10, 12, 14, 15, 16, 17
+    NEAR, FAR, X, GMID, GINN, WVG, WO, RESP, GV, PAR1, PAR2, OMID = 0, 2, 4, 5, 6, 7, 9, 11, 13, 14, 15, 16
+    FORTH, BACK = 20, 21
     sent = []
 
     def remote(k, src, dst, device):
@@ -114,7 +120,7 @@
         else:
             pl.when(when)(copy.start)
         if when is not later:
-            sent.append(copy)
+            sent.append((None if when is early else when, copy))
 
     def share(ref, k, l, when=None):
         to_partner(k + l, ref.at[l, c], ref.at[l, c], when)
@@ -155,7 +161,9 @@
                 gsb[l, h, lanes] = column(gv[h, 1, l : l + 1, lanes])
 
     def prepare_gates():
-        loaded("groups", "ng", "w0")
+        loaded("groups")
+        spread_groups(c)
+        loaded("ng", "w0")
         scale_weights(0)
 
     def prepare_taps():
@@ -179,7 +187,6 @@
         for l in range(layers):
             respond(l)
         prepare_weights()
-        spread_groups(c)
 
     @pl.when(c == 0)
     def _():
@@ -224,11 +231,11 @@
         value = r[:BLK] * kept
         return (value * jnp.tanh(r[BLK:] * inverse) + value).astype(BF16)
 
-    def gate(l, lanes, dst, exists=None, arrived=None):
+    def gate(l, lanes, dst, exists=None, arrived=None, halves=(0, 1)):
         x = xs[:, :, lanes].reshape(features, lanes.stop - lanes.start)
         inverse = half_inverse(squares(x))
         kept = inverse if exists is None else inverse * exists
-        for h in range(2) if arrived is None else (c, p):
+        for h in halves if arrived is None else (c, p):
             if h is p:
                 arrived()
             for k in range(2):
@@ -239,11 +246,15 @@
         n = outputs.stop - outputs.start
         for h in halves:
             w = window(h)
-            g = jnp.dot(w, fwd[: w.shape[1]], preferred_element_type=F32)
-            gr, gi = g[:, :HALF], g[:, HALF:]
-            hr, hi = resp[l, h, :, :HALF].astype(F32), resp[l, h, :, HALF:].astype(F32)
-            y = jnp.concatenate([(gr * hr + gi * hi).astype(BF16), (gi * hr - gr * hi).astype(BF16)], axis=1)
-            filtered = jnp.dot(y, back[:, outputs], preferred_element_type=F32)
+            filtered = None
+            for q in range(2):
+                both, re, im = (slice(2 * q * BLK + i * BLK, 2 * q * BLK + j * BLK) for i, j in ((0, 2), (0, 1), (1, 2)))
+                g = jnp.dot(w, fwd[: w.shape[1], both], preferred_element_type=F32)
+                gr, gi = g[:, :BLK], g[:, BLK:]
+                hr, hi = resp[l, h, :, re].astype(F32), resp[l, h, :, im].astype(F32)
+                y = jnp.concatenate([(gr * hr + gi * hi).astype(BF16), (gi * hr - gr * hi).astype(BF16)], axis=1)
+                term = jnp.dot(y, back[both, outputs], preferred_element_type=F32)
+                filtered = term if filtered is None else filtered + term
             for k in range(2):
                 part = slice(k * BLK, (k + 1) * BLK)
                 f = filtered[part]
@@ -283,6 +294,16 @@
     for k in range(2):
         acc[k] = part_dot(c, k)
     total = part_squares(c)
+    near_block = xs.at[(slice(None), *near)]
+    forth = remote(FORTH, near_block, near_block, (sp, p))
+    back_again = remote(BACK, gnear.at[c], g1.at[(c, *near)], (sp, p))
+
+    @pl.when(early)
+    def _():
+        from_outer(NEAR, lambda core: xs.at[(core, *near)])
+        forth.start()
+        gate(0, outside, g1, halves=(c,))
+
     from_partner(X, xall.at[p])
     inverse = half_inverse(total + part_squares(p))
     for k in range(2):
@@ -304,7 +325,7 @@
     share(resp, RESP, 0, later)
     pl.when(later)(prepare_weights)
     share(wvg, WVG, 1)
-    share(wvg, WVG, 0)
+    share(wvg, WVG, 0, past)
     for h in range(2):
         xs[h, :, BLK : 2 * BLK] = xall[h, 3 * c]
         xs[h, :, 2 * BLK : 3 * BLK] = xall[h, 1 + c]
@@ -314,14 +335,19 @@
 
     loaded("fwd", "back")
 
-    @pl.when(later)
-    def _():
-        spread_groups(c)
-
     inner_window = lambda h: jnp.concatenate([g1[h, :, own], gpar1[h]], axis=1)
     filter_norm(0, inner_window, slice(0, BLK), inner, (c,))
     from_partner(GV, gv.at[p])
     spread_groups(p)
+
+    @pl.when(head)
+    def _():
+        forth.wait_recv()
+        gate(0, outside, gnear, halves=(c,))
+        back_again.start()
+
+    loaded("wo1")
+    share(wo, WO, 1)
 
     from_partner(RESP, resp.at[0, p])
     from_partner(WO, wo.at[0, p])
@@ -330,22 +356,24 @@
     from_partner(GMID, g1.at[p, :, mid])
     filter_norm(0, inner_window, slice(0, BLK), inner, (p,))
     advance(0, inner)
-    from_partner(WVG + 1, wvg.at[1, p])
-    gate(1, inner, g2)
+    gate(1, inner, g2, arrived=lambda: from_partner(WVG + 1, wvg.at[1, p]))
     to_partner(PAR2, g2.at[:, :, inn], gpar2)
     pl.when(later)(lambda: respond(1))
     share(resp, RESP, 1, later)
-    loaded("wo1")
-    share(wo, WO, 1)
-
-    @pl.when(has_outer)
+
+    @pl.when(early)
+    def _():
+        from_partner(BACK, g1.at[(p, *near)])
+        forth.wait_send()
+
+    @pl.when(jnp.logical_and(has_outer, past))
     def _():
         from_outer(NEAR, lambda core: xs.at[(core, *near)])
         gate(0, outside, g1, arrived=lambda: from_partner(WVG, wvg.at[0, p]))
 
     @pl.when(jnp.logical_not(has_outer))
     def _():
-        from_partner(WVG, wvg.at[0, p])
+        pl.when(past)(lambda: from_partner(WVG, wvg.at[0, p]))
         xs[:, :, outside] = jnp.zeros((2, xs.shape[1], BLK), BF16)
         g1[:, :, outside] = jnp.zeros_like(gfar)
         gfar[...] = jnp.zeros_like(gfar)
@@ -368,9 +396,8 @@
         pl.ds(pl.multiple_of((1 + core) * BLK, BLK), BLK),
     )
     whole = slice(0, 2 * BLK)
-    pairs = [tuple((2 * q * BLK + r * BLK, BLK) for r in range(2)) for q in range(2)]
+    project_out(1, p, own, obuf.at[0], whole)
     for q in range(2):
-        project_out(1, p, own, obuf.at[0], whole, pairs[q])
         part = pl.ds(2 * q * BLK, 2 * BLK)
         for k, lane in enumerate(columns(c)):
             to_partner(OMID + 2 * q + k, obuf.at[0, part, pl.ds(k * BLK, BLK)], o_ref.at[part, lane])
@@ -380,8 +407,12 @@
     for copies in (near_copies, far_copies):
         for there, copy in zip((has_left, has_right), copies):
             pl.when(there)(copy.wait_send)
-    for copy in sent:
-        copy.wait_send()
+    for when, copy in sent:
+        if when is None:
+            copy.wait_send()
+        else:
+            pl.when(when)(copy.wait_send)
+    pl.when(head)(back_again.wait_send)
     for q in range(2):
         part = pl.ds(2 * q * BLK, 2 * BLK)
         for k, lane in enumerate(columns(p)):
@@ -392,7 +423,7 @@
     pl.run_scoped(
         lambda *semaphores: kernel(n_sp, *refs, *semaphores),
         pltpu.SemaphoreType.DMA((11,)),
-        pltpu.SemaphoreType.DMA((21,)),
+        pltpu.SemaphoreType.DMA((22,)),
     )
 
 
@@ -450,9 +481,10 @@
                 vmem((2, channels, BLK), BF16),
                 vmem((2, channels, BLK), BF16),
                 vmem((2, channels, BLK), BF16),
+                vmem((2, channels, BLK), BF16),
                 vmem((2, channels, 3 * BLK), BF16),
                 vmem((2, half_features, 2 * BLK), BF16),
-                pltpu.SemaphoreType.DMA((21,)),
+                pltpu.SemaphoreType.DMA((22,)),
                 pltpu.SemaphoreType.REGULAR,
             ],
             compiler_params=pltpu.CompilerParams(

time: 20.4 us -> 19.5 us (0.956)
  the two profiles are of different devices: /device:TPU:1 before, /device:TPU:385 now
where the time goes in v6:
time: 19.5 us; the launch traced here: 19.4 us
  Pallas kernels  19.3 us (99%)
    pallas_call x1, Pallas kernels, body(): pl.pallas_call(functools.partial(scoped, n_sp), out_shape=pltpu.VMEM(stre...  18.5 us
    pallas_call x1, Pallas kernels, write_out(): pl.pallas_call(write_kernel, out_shape=jax.ShapeDtypeStruct(value.shape,...  0.8 us

profile of v6, /device:TPU:385, one launch (start us, length us, event | category | flops | bytes accessed | tf_op | source)
XLA Modules:
  0.0 19.4 jit_solution(15535212529179108849)
XLA Ops:
  0.0 18.5 %shard_map.109.src = bf16[512,512]{1,0:T(8,128)(2,1)S(1)} custom-call(bf16[512,512]{1,0:T(8,128)(2,1)} %refs_0_.1, f32[2,1024]{1,0:T(2,128)} %refs_1_.1, bf16[2,256,1024]{2,1,0:T(8,128)(2,1)} %refs_2_.1, bf16[2,256,1024]{2,1,0:T(8,128)(2,1)} %refs_3_.1, bf16[255,2,256]{2,1,0:T(2,128)(2,1)} %bitcast.1, f32[2,256]{1,0:T(2,128)} %refs_5_.1, f32[2,256]{1,0:T(2,128)} %refs_6_.1, ...), custom_call_target="tpu_custom_call" | custom-call | tf_op jit(solution)/shard_map/pallas_call | solution.py:457
  18.6 0.8 %shard_map.110 = bf16[512,512]{1,0:T(8,128)(2,1)} custom-call(bf16[512,512]{1,0:T(8,128)(2,1)S(1)} %shard_map.109.src), custom_call_target="tpu_custom_call" | custom-call | tf_op jit(solution)/shard_map/pallas_call | solution.py:437

commit v7 on v6

--- a/solution.py
+++ b/solution.py
@@ -45,7 +45,7 @@
     x_hbm, ng_hbm, wv_hbm, wg_hbm, taps_hbm, gg_hbm, gs_hbm, wo_hbm, fwd_hbm, back_hbm, ftap_hbm,
     o_ref,
     xall, xs, wraw, wvg, wo, taps, ngv, gv, ggb, gsb, resp, fwd, back, ftap,
-    acc, gall, g1, g2, gfar, gnear, gpar1, gpar2, act, obuf,
+    acc, begun, gall, g1, g2, gfar, gnear, gpar1, gpar2, act, obuf,
     rsem, ready, lsem, ssem,
 ):
     sp, c = lax.axis_index("sp"), lax.axis_index("tp")
@@ -82,7 +82,7 @@
             pairs.append((wg_hbm.at[l, pl.ds(k * BLK, BLK)], wraw.at[l, k, 1]))
         load(f"w{l}", pairs, wraw.at[l])
 
-    load("x", [(x_hbm.at[:, pl.ds(b * BLK, BLK)], xall.at[c, b]) for b in range(4)], xall.at[c])
+    load("x", [(x_hbm, xall.at[c])], xall.at[c])
 
     barrier = pltpu.get_barrier_semaphore()
     pl.semaphore_signal(barrier, inc=1, device_id=(sp, p), device_id_type=MESH)
@@ -210,7 +210,7 @@
         pl.semaphore_wait(ready, 1)
 
     near = (slice(None), pl.ds(0, BLK))
-    near_copies = [to_neighbour(NEAR, d, xall.at[c, 3 * d], xs.at[(c, *near)]) for d in range(2)]
+    near_copies = [to_neighbour(NEAR, d, xall.at[c, :, pl.ds(3 * d * BLK, BLK)], xs.at[(c, *near)]) for d in range(2)]
     start_both(near_copies)
 
     pl.when(later)(prepare_gates)
@@ -242,7 +242,13 @@
                 r = jnp.dot(wvg[l, h, k].reshape(2 * BLK, features), x, preferred_element_type=F32)
                 dst[h, k * BLK : (k + 1) * BLK, lanes] = gated(r, inverse, kept)
 
-    def filter_norm(l, window, outputs, lanes, halves=(0, 1)):
+    def begin_filter(ready):
+        for h in range(2):
+            for q in range(2):
+                both = slice(2 * q * BLK, 2 * (q + 1) * BLK)
+                begun[h, :, both] = jnp.dot(ready(h), fwd[2 * BLK :, both], preferred_element_type=F32)
+
+    def filter_norm(l, window, outputs, lanes, halves=(0, 1), is_begun=False):
         n = outputs.stop - outputs.start
         for h in halves:
             w = window(h)
@@ -250,6 +256,8 @@
             for q in range(2):
                 both, re, im = (slice(2 * q * BLK + i * BLK, 2 * q * BLK + j * BLK) for i, j in ((0, 2), (0, 1), (1, 2)))
                 g = jnp.dot(w, fwd[: w.shape[1], both], preferred_element_type=F32)
+                if is_begun:
+                    g = g + begun[h, :, both]
                 gr, gi = g[:, :BLK], g[:, BLK:]
                 hr, hi = resp[l, h, :, re].astype(F32), resp[l, h, :, im].astype(F32)
                 y = jnp.concatenate([(gr * hr + gi * hi).astype(BF16), (gi * hr - gr * hi).astype(BF16)], axis=1)
@@ -270,26 +278,33 @@
     def project_out(l, h, lanes, dst, dst_lanes, pieces=((0, 2 * BLK), (2 * BLK, 2 * BLK))):
         for first, size in pieces:
             part = slice(first, first + size)
-            activated = act[:, :, lanes].reshape(wo.shape[3], lanes.stop - lanes.start)
-            branch = jnp.dot(wo[l, h, part], activated, preferred_element_type=F32)
+            branch = None
+            for g in range(2):
+                group = slice(g * 2 * BLK, (g + 1) * 2 * BLK)
+                term = jnp.dot(wo[l, h, part, group], act[g, :, lanes], preferred_element_type=F32)
+                branch = term if branch is None else branch + term
             dst[part, dst_lanes] = (xs[h, part, lanes].astype(F32) + branch).astype(BF16)
 
     def advance(l, lanes):
         for h in range(2):
             project_out(l, h, lanes, xs.at[h], lanes)
 
+    columns = lambda core: (
+        pl.ds(pl.multiple_of(core * 3 * BLK, BLK), BLK),
+        pl.ds(pl.multiple_of((1 + core) * BLK, BLK), BLK),
+    )
     own, outside = slice(BLK, 3 * BLK), slice(0, BLK)
     inner, outward = slice(2 * BLK, 3 * BLK), slice(0, 2 * BLK)
 
     part_rows = features // 2
 
     def part_dot(core, k):
-        x = jnp.concatenate([xall[core, b] for b in range(4)], axis=1)
+        x = xall[core]
         w = wvg[0, c, k, :, :, pl.ds(pl.multiple_of(core * part_rows, part_rows), part_rows)]
         return jnp.dot(w.reshape(2 * BLK, part_rows), x, preferred_element_type=F32)
 
     def part_squares(core):
-        return jnp.concatenate([squares(xall[core, b]) for b in range(4)], axis=1)
+        return squares(xall[core])
 
     for k in range(2):
         acc[k] = part_dot(c, k)
@@ -327,8 +342,8 @@
     share(wvg, WVG, 1)
     share(wvg, WVG, 0, past)
     for h in range(2):
-        xs[h, :, BLK : 2 * BLK] = xall[h, 3 * c]
-        xs[h, :, 2 * BLK : 3 * BLK] = xall[h, 1 + c]
+        for place, lane in zip((1, 2), columns(c)):
+            xs[h, :, place * BLK : (place + 1) * BLK] = xall[h, :, lane]
     g1[c, :, BLK : 2 * BLK] = gall[3 * c]
     g1[c, :, 2 * BLK : 3 * BLK] = gall[1 + c]
     gpar1[c] = gall[1 + p]
@@ -356,7 +371,11 @@
     from_partner(GMID, g1.at[p, :, mid])
     filter_norm(0, inner_window, slice(0, BLK), inner, (p,))
     advance(0, inner)
-    gate(1, inner, g2, arrived=lambda: from_partner(WVG + 1, wvg.at[1, p]))
+    def layer_1_weights():
+        begin_filter(lambda h: g1[h, :, own])
+        from_partner(WVG + 1, wvg.at[1, p])
+
+    gate(1, inner, g2, arrived=layer_1_weights)
     to_partner(PAR2, g2.at[:, :, inn], gpar2)
     pl.when(later)(lambda: respond(1))
     share(resp, RESP, 1, later)
@@ -382,7 +401,9 @@
     def _():
         from_outer(FAR, lambda core: gfar.at[core])
 
-    filter_norm(0, lambda h: jnp.concatenate([gfar[h], g1[h]], axis=1), slice(0, 2 * BLK), outward)
+    filter_norm(
+        0, lambda h: jnp.concatenate([gfar[h], g1[h, :, outside]], axis=1), slice(0, 2 * BLK), outward, is_begun=True
+    )
     advance(0, outward)
     exists = jnp.where(has_outer, 1.0, 0.0)
     gate(1, outward, g2, jnp.concatenate([jnp.full((1, BLK), exists, F32), jnp.ones((1, BLK), F32)], axis=1))
@@ -391,10 +412,6 @@
     from_partner(WO + 1, wo.at[1, p])
     filter_norm(1, lambda h: jnp.concatenate([g2[h], gpar2[h]], axis=1), slice(0, 2 * BLK), own)
 
-    columns = lambda core: (
-        pl.ds(pl.multiple_of(core * 3 * BLK, BLK), BLK),
-        pl.ds(pl.multiple_of((1 + core) * BLK, BLK), BLK),
-    )
     whole = slice(0, 2 * BLK)
     project_out(1, p, own, obuf.at[0], whole)
     for q in range(2):
@@ -460,7 +477,7 @@
             in_specs=[any_spec] * 11,
             out_specs=pl.BlockSpec(memory_space=pltpu.VMEM),
             scratch_shapes=[
-                vmem((2, 4, half_features, BLK), BF16),
+                vmem((2, half_features, tokens), BF16),
                 vmem((2, half_features, 3 * BLK), BF16),
                 vmem((layers, 2, 2, BLK, features), BF16),
                 vmem((layers, 2, 2, 2, BLK, features), BF16),
@@ -475,6 +492,7 @@
                 vmem((SIZE, 2 * BLK), BF16),
                 vmem((layers, SIZE, SIZE), BF16),
                 vmem((2, 2 * BLK, tokens), F32),
+                vmem((2, channels, SIZE), F32),
                 vmem((4, channels, BLK), BF16),
                 vmem((2, channels, 3 * BLK), BF16),
                 vmem((2, channels, 3 * BLK), BF16),

time: 19.5 us -> 19.4 us (level)
  the two profiles are of different devices: /device:TPU:385 before, /device:TPU:1 now
where the time goes in v7:
time: 19.4 us; the launch traced here: 19.2 us
  Pallas kernels  19.2 us (99%)
    pallas_call x1, Pallas kernels, body(): pl.pallas_call(functools.partial(scoped, n_sp), out_shape=pltpu.VMEM(stre...  18.4 us
    pallas_call x1, Pallas kernels, write_out(): pl.pallas_call(write_kernel, out_shape=jax.ShapeDtypeStruct(value.shape,...  0.8 us

profile of v7, /device:TPU:1, one launch (start us, length us, event | category | flops | bytes accessed | tf_op | source)
XLA Modules:
  0.0 19.2 jit_solution(6440257684446633808)
XLA Ops:
  0.0 18.4 %shard_map.109.src = bf16[512,512]{1,0:T(8,128)(2,1)S(1)} custom-call(bf16[512,512]{1,0:T(8,128)(2,1)} %refs_0_.1, f32[2,1024]{1,0:T(2,128)} %refs_1_.1, bf16[2,256,1024]{2,1,0:T(8,128)(2,1)} %refs_2_.1, bf16[2,256,1024]{2,1,0:T(8,128)(2,1)} %refs_3_.1, bf16[255,2,256]{2,1,0:T(2,128)(2,1)} %bitcast.1, f32[2,256]{1,0:T(2,128)} %refs_5_.1, f32[2,256]{1,0:T(2,128)} %refs_6_.1, ...), custom_call_target="tpu_custom_call" | custom-call | tf_op jit(solution)/shard_map/pallas_call | solution.py:474
  18.4 0.8 %shard_map.110 = bf16[512,512]{1,0:T(8,128)(2,1)} custom-call(bf16[512,512]{1,0:T(8,128)(2,1)S(1)} %shard_map.109.src), custom_call_target="tpu_custom_call" | custom-call | tf_op jit(solution)/shard_map/pallas_call | solution.py:454

commit v8 on v7

--- a/solution.py
+++ b/solution.py
@@ -45,7 +45,7 @@
     x_hbm, ng_hbm, wv_hbm, wg_hbm, taps_hbm, gg_hbm, gs_hbm, wo_hbm, fwd_hbm, back_hbm, ftap_hbm,
     o_ref,
     xall, xs, wraw, wvg, wo, taps, ngv, gv, ggb, gsb, resp, fwd, back, ftap,
-    acc, begun, gall, g1, g2, gfar, gnear, gpar1, gpar2, act, obuf,
+    acc, begun, begun_last, gall, g1, g2, gfar, gnear, gpar1, gpar2, act, obuf,
     rsem, ready, lsem, ssem,
 ):
     sp, c = lax.axis_index("sp"), lax.axis_index("tp")
@@ -59,6 +59,8 @@
     early = jnp.logical_and(first, c == 1)
     later = jnp.logical_not(early)
     past = sp > 0
+    slow = jnp.logical_and(past, lax.rem(sp, 16) == 0)
+    prompt = jnp.logical_not(slow)
     left_count = jnp.where(has_left, 1, 0)
     right_count = jnp.where(has_right, 1, 0)
     layers, features = ng_hbm.shape
@@ -199,6 +201,16 @@
 
     loaded("x")
     to_partner(X, xall.at[c], xall.at[c])
+    wo_copy = remote(WO, wo.at[0, c], wo.at[0, c], (sp, p))
+    wvg_copy = remote(WVG, wvg.at[0, c], wvg.at[0, c], (sp, p))
+    sent.extend([(None, wo_copy), (past, wvg_copy)])
+
+    @pl.when(slow)
+    def _():
+        loaded("wo0")
+        wo_copy.start()
+        prepare_gates()
+        wvg_copy.start()
 
     @pl.when(c == 1)
     def _():
@@ -213,10 +225,14 @@
     near_copies = [to_neighbour(NEAR, d, xall.at[c, :, pl.ds(3 * d * BLK, BLK)], xs.at[(c, *near)]) for d in range(2)]
     start_both(near_copies)
 
-    pl.when(later)(prepare_gates)
+    pl.when(jnp.logical_and(later, prompt))(prepare_gates)
     to_partner(GV, gv.at[c], gv.at[c])
-    loaded("wo0")
-    share(wo, WO, 0)
+
+    @pl.when(prompt)
+    def _():
+        loaded("wo0")
+        wo_copy.start()
+
     for l in range(layers):
         share(resp, RESP, l, early)
 
@@ -227,28 +243,27 @@
     def half_inverse(total):
         return 0.5 * lax.rsqrt(total * (1.0 / features) + RMS_EPS)
 
-    def gated(r, inverse, kept):
-        value = r[:BLK] * kept
+    def gated(r, inverse):
+        value = r[:BLK] * inverse
         return (value * jnp.tanh(r[BLK:] * inverse) + value).astype(BF16)
 
-    def gate(l, lanes, dst, exists=None, arrived=None, halves=(0, 1)):
+    def gate(l, lanes, dst, arrived=None, halves=(0, 1)):
         x = xs[:, :, lanes].reshape(features, lanes.stop - lanes.start)
         inverse = half_inverse(squares(x))
-        kept = inverse if exists is None else inverse * exists
         for h in halves if arrived is None else (c, p):
             if h is p:
                 arrived()
             for k in range(2):
                 r = jnp.dot(wvg[l, h, k].reshape(2 * BLK, features), x, preferred_element_type=F32)
-                dst[h, k * BLK : (k + 1) * BLK, lanes] = gated(r, inverse, kept)
-
-    def begin_filter(ready):
+                dst[h, k * BLK : (k + 1) * BLK, lanes] = gated(r, inverse)
+
+    def begin_filter(begun, ready):
         for h in range(2):
             for q in range(2):
                 both = slice(2 * q * BLK, 2 * (q + 1) * BLK)
                 begun[h, :, both] = jnp.dot(ready(h), fwd[2 * BLK :, both], preferred_element_type=F32)
 
-    def filter_norm(l, window, outputs, lanes, halves=(0, 1), is_begun=False):
+    def filter_norm(l, window, outputs, lanes, halves=(0, 1), begun=None):
         n = outputs.stop - outputs.start
         for h in halves:
             w = window(h)
@@ -256,7 +271,7 @@
             for q in range(2):
                 both, re, im = (slice(2 * q * BLK + i * BLK, 2 * q * BLK + j * BLK) for i, j in ((0, 2), (0, 1), (1, 2)))
                 g = jnp.dot(w, fwd[: w.shape[1], both], preferred_element_type=F32)
-                if is_begun:
+                if begun is not None:
                     g = g + begun[h, :, both]
                 gr, gi = g[:, :BLK], g[:, BLK:]
                 hr, hi = resp[l, h, :, re].astype(F32), resp[l, h, :, im].astype(F32)
@@ -322,7 +337,7 @@
     from_partner(X, xall.at[p])
     inverse = half_inverse(total + part_squares(p))
     for k in range(2):
-        gk = gated(acc[k] + part_dot(p, k), inverse, inverse)
+        gk = gated(acc[k] + part_dot(p, k), inverse)
         for b in range(4):
             gall[b, k * BLK : (k + 1) * BLK] = gk[:, b * BLK : (b + 1) * BLK]
     mid, inn = pl.ds(BLK, BLK), pl.ds(2 * BLK, BLK)
@@ -340,7 +355,7 @@
     share(resp, RESP, 0, later)
     pl.when(later)(prepare_weights)
     share(wvg, WVG, 1)
-    share(wvg, WVG, 0, past)
+    pl.when(jnp.logical_and(past, prompt))(wvg_copy.start)
     for h in range(2):
         for place, lane in zip((1, 2), columns(c)):
             xs[h, :, place * BLK : (place + 1) * BLK] = xall[h, :, lane]
@@ -351,7 +366,13 @@
     loaded("fwd", "back")
 
     inner_window = lambda h: jnp.concatenate([g1[h, :, own], gpar1[h]], axis=1)
-    filter_norm(0, inner_window, slice(0, BLK), inner, (c,))
+    alone = jnp.logical_not(has_outer)
+    inside = jnp.logical_and(has_outer, past)
+
+    @pl.when(has_outer)
+    def _():
+        filter_norm(0, inner_window, slice(0, BLK), inner, (c,))
+
     from_partner(GV, gv.at[p])
     spread_groups(p)
 
@@ -360,57 +381,66 @@
         forth.wait_recv()
         gate(0, outside, gnear, halves=(c,))
         back_again.start()
-
-    loaded("wo1")
-    share(wo, WO, 1)
 
     from_partner(RESP, resp.at[0, p])
     from_partner(WO, wo.at[0, p])
     from_partner(GINN, g1.at[p, :, inn])
     from_partner(PAR1, gpar1.at[p])
     from_partner(GMID, g1.at[p, :, mid])
-    filter_norm(0, inner_window, slice(0, BLK), inner, (p,))
-    advance(0, inner)
-    def layer_1_weights():
-        begin_filter(lambda h: g1[h, :, own])
+
+    @pl.when(has_outer)
+    def _():
+        def layer_1_weights():
+            begin_filter(begun, lambda h: g1[h, :, own])
+            from_partner(WVG + 1, wvg.at[1, p])
+
+        filter_norm(0, inner_window, slice(0, BLK), inner, (p,))
+        advance(0, inner)
+        gate(1, inner, g2, arrived=layer_1_weights)
+
+    @pl.when(alone)
+    def _():
+        pl.when(past)(lambda: from_partner(WVG, wvg.at[0, p]))
+        g1[:, :, outside] = jnp.zeros_like(gfar)
+        filter_norm(0, lambda h: jnp.concatenate([g1[h], gpar1[h]], axis=1), slice(0, 2 * BLK), own)
+        advance(0, own)
         from_partner(WVG + 1, wvg.at[1, p])
-
-    gate(1, inner, g2, arrived=layer_1_weights)
+        gate(1, own, g2)
+        g2[:, :, outside] = jnp.zeros_like(gfar)
+
     to_partner(PAR2, g2.at[:, :, inn], gpar2)
     pl.when(later)(lambda: respond(1))
     share(resp, RESP, 1, later)
+    loaded("wo1")
+    share(wo, WO, 1)
+
+    def begin_last():
+        from_partner(PAR2, gpar2)
+        begin_filter(begun_last, lambda h: jnp.concatenate([g2[h, :, inner], gpar2[h]], axis=1))
 
     @pl.when(early)
     def _():
         from_partner(BACK, g1.at[(p, *near)])
         forth.wait_send()
 
-    @pl.when(jnp.logical_and(has_outer, past))
+    @pl.when(inside)
     def _():
         from_outer(NEAR, lambda core: xs.at[(core, *near)])
         gate(0, outside, g1, arrived=lambda: from_partner(WVG, wvg.at[0, p]))
-
-    @pl.when(jnp.logical_not(has_outer))
-    def _():
-        pl.when(past)(lambda: from_partner(WVG, wvg.at[0, p]))
-        xs[:, :, outside] = jnp.zeros((2, xs.shape[1], BLK), BF16)
-        g1[:, :, outside] = jnp.zeros_like(gfar)
-        gfar[...] = jnp.zeros_like(gfar)
+        begin_last()
 
     @pl.when(has_outer)
     def _():
         from_outer(FAR, lambda core: gfar.at[core])
-
-    filter_norm(
-        0, lambda h: jnp.concatenate([gfar[h], g1[h, :, outside]], axis=1), slice(0, 2 * BLK), outward, is_begun=True
-    )
-    advance(0, outward)
-    exists = jnp.where(has_outer, 1.0, 0.0)
-    gate(1, outward, g2, jnp.concatenate([jnp.full((1, BLK), exists, F32), jnp.ones((1, BLK), F32)], axis=1))
-    from_partner(PAR2, gpar2)
+        late = lambda h: jnp.concatenate([gfar[h], g1[h, :, outside]], axis=1)
+        filter_norm(0, late, slice(0, 2 * BLK), outward, begun=begun)
+        advance(0, outward)
+        gate(1, outward, g2)
+
+    pl.when(jnp.logical_not(inside))(begin_last)
     from_partner(RESP + 1, resp.at[1, p])
+    filter_norm(1, lambda h: g2[h, :, outward], slice(0, 2 * BLK), own, begun=begun_last)
     from_partner(WO + 1, wo.at[1, p])
-    filter_norm(1, lambda h: jnp.concatenate([g2[h], gpar2[h]], axis=1), slice(0, 2 * BLK), own)
 
     whole = slice(0, 2 * BLK)
     project_out(1, p, own, obuf.at[0], whole)
@@ -493,6 +523,7 @@
                 vmem((layers, SIZE, SIZE), BF16),
                 vmem((2, 2 * BLK, tokens), F32),
                 vmem((2, channels, SIZE), F32),
+                vmem((2, channels, SIZE), F32),
                 vmem((4, channels, BLK), BF16),
                 vmem((2, channels, 3 * BLK), BF16),
                 vmem((2, channels, 3 * BLK), BF16),

time: 19.4 us -> 19.4 us (level)
  the two profiles are of different devices: /device:TPU:1 before, /device:TPU:129 now
where the time goes in v8:
time: 19.4 us; the launch traced here: 19.3 us
  Pallas kernels  19.3 us (99%)
    pallas_call x1, Pallas kernels, body(): pl.pallas_call(functools.partial(scoped, n_sp), out_shape=pltpu.VMEM(stre...  18.4 us
    pallas_call x1, Pallas kernels, write_out(): pl.pallas_call(write_kernel, out_shape=jax.ShapeDtypeStruct(value.shape,...  0.8 us

profile of v8, /device:TPU:129, one launch (start us, length us, event | category | flops | bytes accessed | tf_op | source)
XLA Modules:
  0.0 19.3 jit_solution(704411961368653921)
XLA Ops:
  0.0 18.4 %shard_map.109.src = bf16[512,512]{1,0:T(8,128)(2,1)S(1)} custom-call(bf16[512,512]{1,0:T(8,128)(2,1)} %refs_0_.1, f32[2,1024]{1,0:T(2,128)} %refs_1_.1, bf16[2,256,1024]{2,1,0:T(8,128)(2,1)} %refs_2_.1, bf16[2,256,1024]{2,1,0:T(8,128)(2,1)} %refs_3_.1, bf16[255,2,256]{2,1,0:T(2,128)(2,1)} %bitcast.1, f32[2,256]{1,0:T(2,128)} %refs_5_.1, f32[2,256]{1,0:T(2,128)} %refs_6_.1, ...), custom_call_target="tpu_custom_call" | custom-call | tf_op jit(solution)/shard_map/pallas_call | solution.py:504
  18.5 0.8 %shard_map.110 = bf16[512,512]{1,0:T(8,128)(2,1)} custom-call(bf16[512,512]{1,0:T(8,128)(2,1)S(1)} %shard_map.109.src), custom_call_target="tpu_custom_call" | custom-call | tf_op jit(solution)/shard_map/pallas_call | solution.py:484

commit v9 on v8

--- a/solution.py
+++ b/solution.py
@@ -425,8 +425,9 @@
 
     @pl.when(inside)
     def _():
+        from_partner(WVG, wvg.at[0, p])
         from_outer(NEAR, lambda core: xs.at[(core, *near)])
-        gate(0, outside, g1, arrived=lambda: from_partner(WVG, wvg.at[0, p]))
+        gate(0, outside, g1)
         begin_last()
 
     @pl.when(has_outer)

time: 19.4 us -> 19.2 us (0.990)
  the two profiles are of different devices: /device:TPU:129 before, /device:TPU:257 now
where the time goes in v9:
time: 19.2 us; the launch traced here: 19.1 us
  Pallas kernels  19.1 us (99%)
    pallas_call x1, Pallas kernels, body(): pl.pallas_call(functools.partial(scoped, n_sp), out_shape=pltpu.VMEM(stre...  18.3 us
    pallas_call x1, Pallas kernels, write_out(): pl.pallas_call(write_kernel, out_shape=jax.ShapeDtypeStruct(value.shape,...  0.8 us

profile of v9, /device:TPU:257, one launch (start us, length us, event | category | flops | bytes accessed | tf_op | source)
XLA Modules:
  0.0 19.1 jit_solution(10344833593460950354)
XLA Ops:
  0.0 18.3 %shard_map.109.src = bf16[512,512]{1,0:T(8,128)(2,1)S(1)} custom-call(bf16[512,512]{1,0:T(8,128)(2,1)} %refs_0_.1, f32[2,1024]{1,0:T(2,128)} %refs_1_.1, bf16[2,256,1024]{2,1,0:T(8,128)(2,1)} %refs_2_.1, bf16[2,256,1024]{2,1,0:T(8,128)(2,1)} %refs_3_.1, bf16[255,2,256]{2,1,0:T(2,128)(2,1)} %bitcast.1, f32[2,256]{1,0:T(2,128)} %refs_5_.1, f32[2,256]{1,0:T(2,128)} %refs_6_.1, ...), custom_call_target="tpu_custom_call" | custom-call | tf_op jit(solution)/shard_map/pallas_call | solution.py:505
  18.3 0.8 %shard_map.110 = bf16[512,512]{1,0:T(8,128)(2,1)} custom-call(bf16[512,512]{1,0:T(8,128)(2,1)S(1)} %shard_map.109.src), custom_call_target="tpu_custom_call" | custom-call | tf_op jit(solution)/shard_map/pallas_call | solution.py:485
